TPU v7x, 128 devices: a whole 4x4x4 slice. The times are simulated.
128 devices in a mesh: sp: 16 (over z, x), dp: 8 (over y, core).
Axes of the slice: x: 4, y: 4, z: 4, core: 2. Of those that a mesh axis runs over, the one named last changes fastest.
Arguments:
- queries: bfloat16 [8, 2048, 2048], P('dp', 'sp'), may hold values from -9 to 9
- keys: bfloat16 [8, 2048, 512], P('dp', 'sp'), may hold values from -9 to 9
- values: bfloat16 [8, 2048, 512], P('dp', 'sp'), may hold values from -6 to 6
- out_grad: bfloat16 [8, 2048, 2048], P('dp', 'sp'), may hold values from -24 to 24
- layer_in: bfloat16 [8, 2048, 4096], P('dp', 'sp'), may hold values from -0.09375 to 0.09375
- key_weight: bfloat16 [4096, 512], P('dp'), may hold values from -0.09375 to 0.09375
- value_weight: bfloat16 [4096, 512], P('dp'), may hold values from -0.09375 to 0.09375
- query_gain: float32 [128], replicated, may hold values from 0.64 to 6.04
- key_gain: float32 [128], replicated, may hold values from 0.64 to 6.04
Outputs:
- grad_query: bfloat16 [8, 2048, 2048], P('dp', 'sp')
- grad_in: bfloat16 [8, 2048, 4096], P('dp', 'sp')
- grad_key_weight: float32 [4096, 512], P('dp')
- grad_value_weight: float32 [4096, 512], P('dp')
All inputs are finite; a program needn't handle non-finite values.
Results may differ from a plain program's by a relative error of at most 0.018.
The roundings to bfloat16 on the way count: a program that leaves them out, or rounds other values in their place, can miss the bound.
Values may be sent and summed in bfloat16 or wider, within the bound.
No kernel may reach another device: no remote copies, remote signals or barrier semaphores. Data moves between devices by JAX's collectives and lax.ppermute only.
A program may use at most 128 MiB of HBM per device.

v0:
```python
import math

import jax
import jax.numpy as jnp
import numpy as np
from jax import lax
from jax.experimental import pallas as pl
from jax.experimental.pallas import tpu as pltpu
from jax.sharding import Mesh
from jax.sharding import PartitionSpec as P


HEAD_DIM = 128
GRID_W = 64
TOK = 128
LEN = 2048
NZ = 4
NX = 4
NY = 4
GROUP_COLS = 512
epsilon = 1e-06
rope_base = 10000.0

F32 = jnp.float32
BF = jnp.bfloat16
SCALE = HEAD_DIM**-0.5
EXP2_SCALE = SCALE * math.log2(math.e)
CHUNK = 512


def rope_tables():
    quarter = HEAD_DIM // 4
    lane = np.arange(HEAD_DIM)
    out = []
    for count, mine in ((LEN // GRID_W, lane < 64), (GRID_W, lane >= 64)):
        shape = (count, HEAD_DIM)
        place = lax.broadcasted_iota(jnp.int32, shape, 1)
        freq = rope_base ** (-(place % quarter).astype(F32) / quarter)
        turn = lax.broadcasted_iota(jnp.int32, shape, 0).astype(F32) * freq
        keep = (place < 64) if mine[0] else (place >= 64)
        sin = jnp.where(place % 64 < quarter, -jnp.sin(turn), jnp.sin(turn))
        out.append(jnp.where(keep, jnp.cos(turn), 0.0))
        out.append(jnp.where(keep, sin, 0.0))
    return out


VMEM = pl.BlockSpec(memory_space=pltpu.VMEM)


def call(body, outs, args, scratch=(), flops=0, nbytes=1 << 20, limit=12):
    return pl.pallas_call(
        body,
        out_shape=[jax.ShapeDtypeStruct(s, d) for s, d in outs],
        in_specs=[VMEM] * len(args),
        out_specs=[VMEM] * len(outs),
        scratch_shapes=list(scratch),
        cost_estimate=pl.CostEstimate(flops=flops, bytes_accessed=nbytes, transcendentals=0),
        compiler_params=pltpu.CompilerParams(vmem_limit_bytes=limit << 20),
    )(*args)


def axis(name):
    return lax.axis_index(name)


def cyc(i):
    return lax.rem(i, 4)


def span(index, size):
    return pl.ds(pl.multiple_of(index * size, size), size)


def angles(tables, z):
    first = 2 * (4 * z + axis("x"))
    out = []
    for row_ref, col_ref in (tables[0::2], tables[1::2]):
        halves = [row_ref[pl.ds(first + r, 1), :] + col_ref[...] for r in range(2)]
        out.append(jnp.concatenate(halves, axis=0))
    return out


def swap_pairs(v):
    lane = lax.broadcasted_iota(jnp.int32, v.shape, 1)
    return jnp.where(lane % 64 < 32, pltpu.roll(v, 96, 1), pltpu.roll(v, 32, 1))


def rms(u):
    return lax.rsqrt(jnp.mean(u * u, axis=1, keepdims=True) + epsilon)


def forward_rotate(u, gain, cos, sin):
    n = u * rms(u) * gain
    return n * cos + swap_pairs(n) * sin


def backward_rotate(g, u, gain, cos, sin):
    r = rms(u)
    w = (g * cos - swap_pairs(g) * sin) * gain
    return r * w - u * (r * r * r * jnp.mean(u * w, axis=1, keepdims=True))


def prep_kv_body(k_ref, v_ref, gain_ref, *refs):
    tables, outs = refs[:4], refs[4:]
    z = axis("z")
    cos, sin = angles(tables, z)
    for s in range(4):
        cols = span(cyc(z + s), HEAD_DIM)
        raw = k_ref[:, cols]
        outs[s][0] = forward_rotate(raw.astype(F32), gain_ref[...], cos, sin).astype(BF)
        outs[s][1] = v_ref[:, cols]
        outs[s][2] = raw


def prep_q_body(q_ref, g_ref, gain_ref, *refs):
    tables, outs = refs[:4], refs[4:]
    z = axis("z")
    cos, sin = angles(tables, z)
    for s in range(4):
        group = cyc(z + s)
        for h in range(4):
            cols = span(4 * group + h, HEAD_DIM)
            rows = pl.ds(h * TOK, TOK)
            u = q_ref[:, cols].astype(F32)
            outs[s][0, rows, :] = forward_rotate(u, gain_ref[...], cos, sin).astype(BF)
            outs[s][1, rows, :] = g_ref[:, cols]


def join_kv_body(*refs):
    kv, raw = refs[4:]
    for s in range(4):
        rows = pl.ds(s * TOK, TOK)
        for k in range(2):
            kv[k, rows, :] = refs[s][k]
        raw[rows, :] = refs[s][2]


def dg(a, b, ca, cb):
    return lax.dot_general(a, b, (((ca,), (cb,)), ((), ())), preferred_element_type=F32)


def attend_body(*refs):
    q_in, kv_in = refs[0:4], refs[4:8]
    dq_out, dk_out, dv_out = refs[8:12], refs[12:16], refs[16:20]
    q_all, g_all, k_all, v_all, dq_all, dk_acc, dv_acc = refs[20:]
    for s in range(4):
        rows = pl.ds(s * 512, 512)
        q_all[rows, :] = q_in[s][0]
        g_all[rows, :] = q_in[s][1]
        k_all[rows, :] = kv_in[s][0]
        v_all[rows, :] = kv_in[s][1]
    dk_acc[...] = jnp.zeros_like(dk_acc)
    dv_acc[...] = jnp.zeros_like(dv_acc)

    def step(i, carry):
        rows = span(i, CHUNK)
        q, g, k, v = q_all[rows, :], g_all[rows, :], k_all[...], v_all[...]
        scores = dg(q, k, 1, 1)
        top = jnp.max(scores, axis=1, keepdims=True)
        e = jnp.exp2((scores - top) * EXP2_SCALE)
        probs = e * (1.0 / jnp.sum(e, axis=1, keepdims=True))
        probs_b = probs.astype(BF)
        grad_probs = dg(g, v, 1, 1)
        delta = jnp.sum(probs_b.astype(F32) * grad_probs, axis=1, keepdims=True)
        grad_scores = (probs * (grad_probs - delta)).astype(BF)
        dq_all[rows, :] = (dg(grad_scores, k, 1, 0) * SCALE).astype(BF)
        dk_acc[...] += dg(q, grad_scores, 0, 0)
        dv_acc[...] += dg(g, probs_b, 0, 0)
        return carry

    lax.fori_loop(0, LEN // CHUNK, step, 0)
    for s in range(4):
        rows = pl.ds(s * 512, 512)
        dq_out[s][...] = dq_all[rows, :]
        dk_out[s][...] = (dk_acc[:, rows].T * SCALE).astype(BF)
        dv_out[s][...] = dv_acc[:, rows].T.astype(BF)


def sum_four(refs, where):
    total = refs[0][where].astype(F32)
    for r in refs[1:4]:
        total = total + r[where].astype(F32)
    return total


def sum_v_body(*refs):
    refs[4][...] = sum_four(refs, (slice(None), slice(None))).astype(BF)


def k_back_body(*refs):
    dq, (v_ref, raw_ref, kg_ref), tables = refs[4:8], refs[8:11], refs[11:15]
    out, msgs = refs[15], refs[16:20]
    z = axis("z")
    for s in range(4):
        rows = pl.ds(s * TOK, TOK)
        cos, sin = angles(tables, cyc(z + 4 - s))
        g = sum_four(refs, (rows, slice(None)))
        u = raw_ref[rows, :].astype(F32)
        k_sum = backward_rotate(g, u, kg_ref[...], cos, sin).astype(BF)
        out[rows, :] = k_sum
        msgs[s][0] = k_sum
        msgs[s][1] = v_ref[rows, :]
        for h in range(4):
            msgs[s][2 + h] = dq[s][pl.ds(h * TOK, TOK), :]


def q_back_body(*refs):
    msgs, (q_ref, qg_ref), tables, out = refs[0:4], refs[4:6], refs[6:10], refs[10]
    z = axis("z")
    cos, sin = angles(tables, z)
    for s in range(4):
        group = cyc(z + s)
        for h in range(4):
            cols = span(4 * group + h, HEAD_DIM)
            u = q_ref[:, cols].astype(F32)
            g = msgs[s][2 + h].astype(F32)
            out[:, cols] = backward_rotate(g, u, qg_ref[...], cos, sin).astype(BF)


def cut_input_body(in_ref, own, sib):
    y, c = axis("y"), axis("c")
    for s in range(4):
        there = cyc(y + s)
        own[s] = in_ref[:, span(2 * there + c, GROUP_COLS)]
        sib[s] = in_ref[:, span(2 * there + 1 - c, GROUP_COLS)]


def weight_body(*refs):
    inputs, own, sib = refs[0:4], refs[4:8], refs[8:12]
    out, right = refs[12:]
    for b in range(4):
        for s in range(4):
            for p, kv in ((0, own), (1, sib)):
                rows = pl.ds(b * 1024 + (2 * s + p) * TOK, TOK)
                right[rows, :] = kv[s][pl.ds(b * TOK, TOK), :]
    total = None
    for b in range(4):
        part = dg(right[pl.ds(b * 1024, 1024), :], inputs[b][...], 0, 0)
        total = part if total is None else total + part
    out[...] = total.astype(BF)


def sum_weight_body(*refs):
    refs[4][...] = sum_four(refs, (slice(None), slice(None))).T.astype(BF)


def place_weight_body(*refs):
    z = axis("z")
    for s in range(4):
        refs[4][:, span(cyc(z + 4 - s), HEAD_DIM)] = refs[s][...].astype(F32)


def input_grad_body(*refs):
    pieces, own, sib = refs[0:4], refs[4:8], refs[8:12]
    out, kv = refs[12:]
    z, y, c = axis("z"), axis("y"), axis("c")
    for s in range(4):
        head = cyc(z + s)
        for k in range(2):
            kv[:, span(4 * k + head, HEAD_DIM)] = pieces[s][k]
    for s in range(4):
        there = cyc(y + 4 - s)
        for w, core in ((own[s], c), (sib[s], 1 - c)):
            both = dg(kv[:, :512], w[0], 1, 1) + dg(kv[:, 512:], w[1], 1, 1)
            out[:, span(2 * there + core, GROUP_COLS)] = both.astype(BF)


def shift(array, name, by):
    n = lax.axis_size(name)
    return lax.ppermute(array, name, [(i, (i + by) % n) for i in range(n)])


def exchange(parts, name, sign=1):
    out = [parts[0]]
    for s in (1, 2, 3):
        out.append(shift(parts[s], name, sign * s))
    return out


def on_device(
    queries, keys, values, out_grad, layer_in, key_weight, value_weight, query_gain, key_gain
):
    return whole(
        *(a[0] for a in (queries, keys, values, out_grad, layer_in)),
        key_weight,
        value_weight,
        query_gain[None],
        key_gain[None],
    )


def whole(queries, keys, values, out_grad, layer_in, key_weight, value_weight, qg, kg):
    square = ((512, 128), BF)
    tables = rope_tables()

    kv_msgs = call(prep_kv_body, [((3, 128, 128), BF)] * 4, (keys, values, kg, *tables))
    kv_pieces = exchange(kv_msgs, "z")
    q_msgs = call(
        prep_q_body, [((2, 512, 128), BF)] * 4, (queries, out_grad, qg, *tables)
    )
    q_parts = exchange(q_msgs, "z")
    kv_here, raw_keys = call(join_kv_body, [((2, 512, 128), BF), square], kv_pieces)
    kv_parts = exchange([kv_here] * 4, "x")

    in_own, in_sib = call(cut_input_body, [((4, 128, 512), BF)] * 2, (layer_in,))
    in_sib = shift(in_sib, "c", 1)
    in_msgs = [None] + [jnp.stack([in_own[s], in_sib[s]]) for s in (1, 2, 3)]
    in_parts = exchange(in_msgs, "y")
    in_first = jnp.stack([in_own[0], in_sib[0]])
    in_all = jnp.stack([in_first, *in_parts[1:]]).reshape(1024, 512)
    inputs = exchange([in_all] * 4, "z")

    weights = jnp.stack([key_weight, value_weight])
    w_prev = shift(weights, "y", 1)
    w_next = shift(weights, "y", -1)
    w_far = jnp.stack([shift(w_prev[0], "y", 1), shift(w_next[1], "y", -1)])
    w_own = [weights, w_prev, w_far, w_next]
    w_sib = [shift(w, "c", 1) for w in w_own]

    attended = call(
        attend_body,
        [square] * 12,
        (*q_parts, *kv_parts),
        scratch=[pltpu.VMEM((LEN, 128), BF)] * 5 + [pltpu.VMEM((128, LEN), F32)] * 2,
        flops=5 * 2 * LEN * LEN * 128,
        nbytes=4 << 20,
        limit=32,
    )
    dq_out, dk_out, dv_out = attended[:4], attended[4:8], attended[8:]
    dv_parts = exchange(dv_out, "x", -1)
    dk_parts = exchange(dk_out, "x", -1)

    (v_sum,) = call(sum_v_body, [square], dv_parts)
    v_own = exchange([v_sum] * 4, "y")
    v_sib = [shift(a, "c", 1) for a in v_own]

    k_sum, *token_grads = call(
        k_back_body,
        [square] + [((6, 128, 128), BF)] * 4,
        (*dk_parts, *dq_out, v_sum, raw_keys, kg, *tables),
    )
    k_own = exchange([k_sum] * 4, "y")
    k_sib = [shift(a, "c", 1) for a in k_own]
    token_grads = exchange(token_grads, "z", -1)

    (grad_query,) = call(
        q_back_body, [((128, 2048), BF)], (*token_grads, queries, qg, *tables)
    )

    def weight_chain(own, sib):
        (part,) = call(
            weight_body,
            [((128, 512), BF)],
            (*inputs, *own, *sib),
            scratch=[pltpu.VMEM((4096, 128), BF)],
            flops=2 * 4096 * 512 * 128,
            limit=16,
        )
        parts = exchange([part] * 4, "x")
        (total,) = call(sum_weight_body, [square], parts)
        blocks = exchange([total] * 4, "z")
        (out,) = call(place_weight_body, [((512, 512), F32)], blocks)
        return out

    grad_value_weight = weight_chain(v_own, v_sib)
    grad_key_weight = weight_chain(k_own, k_sib)
    (grad_in,) = call(
        input_grad_body,
        [((128, 4096), BF)],
        (*token_grads, *w_own, *w_sib),
        scratch=[pltpu.VMEM((128, 1024), BF)],
        flops=2 * 128 * 1024 * 4096,
        nbytes=9 << 20,
        limit=24,
    )
    return (grad_query[None], grad_in[None], grad_key_weight, grad_value_weight)


def solution(mesh):
    cube = Mesh(mesh.devices.reshape(NZ, NX, NY, 2), ("z", "x", "y", "c"))
    sp, dp = ("z", "x"), ("y", "c")
    tokens = P(dp, sp, None)
    weights = P(dp, None)
    return jax.shard_map(
        on_device,
        mesh=cube,
        in_specs=(tokens,) * 5 + (weights,) * 2 + (P(), P()),
        out_specs=(tokens, tokens, weights, weights),
        check_vma=False,
    )
```

profile of v0, /device:TPU:8, one launch (start us, length us, event | category | flops | bytes accessed | tf_op | source)
XLA Modules:
  0.0 252.0 jit_solution(3071056601701613266)
XLA Ops:
  3.8 2.1 shard_map.120
  13.7 2.5 %collective-permute-start.5 = (bf16[3,128,128]{2,1,0:T(8,128)(2,1)S(1)}, bf16[3,128,128]{2,1,0:T(8,128)(2,1)S(1)}, u32[]{:S(2)}, u32[]{:S(2)}) collective-permute-start(bf16[3,128,128]{2,1,0:T(8,128)(2,1)S(1)} %get-tuple-element.40), channel_id=1, source_target_pairs={{0,96},{32,0},{64,32},{96,64},{1,97},{33,1},{65,33},{97,65},{2,98}... | collective-permute-start | bytes 294920 | tf_op jit(solution)/shard_map/ppermute | solution.py:270
  16.3 2.2 collective-permute-done.3.refs_1_
  18.5 2.9 %collective-permute-start.2 = (bf16[2,512,128]{2,1,0:T(8,128)(2,1)S(1)}, bf16[2,512,128]{2,1,0:T(8,128)(2,1)S(1)}, u32[]{:S(2)}, u32[]{:S(2)}) collective-permute-start(bf16[2,512,128]{2,1,0:T(8,128)(2,1)S(1)} %get-tuple-element.36), channel_id=1, source_target_pairs={{0,96},{32,0},{64,32},{96,64},{1,97},{33,1},{65,33},{97,65},{2,98}... | collective-permute-start | bytes 786440 | tf_op jit(solution)/shard_map/ppermute | solution.py:270
  25.1 2.7 %collective-permute-start.7 = (bf16[2,512,128]{2,1,0:T(8,128)(2,1)S(1)}, bf16[2,512,128]{2,1,0:T(8,128)(2,1)S(1)}, u32[]{:S(2)}, u32[]{:S(2)}) collective-permute-start(bf16[2,512,128]{2,1,0:T(8,128)(2,1)S(1)} %get-tuple-element.41.refs_4_), channel_id=1, source_target_pairs={{0,16},{8,24},{16,0},{24,8},{1,17},{9,25},{17,1},{25,9},{2,18},{10... | collective-permute-start | bytes 786440 | tf_op jit(solution)/shard_map/ppermute | solution.py:270
  30.0 3.8 %collective-permute-done.6.refs_5_ = bf16[2,512,128]{2,1,0:T(8,128)(2,1)S(1)} collective-permute-done((bf16[2,512,128]{2,1,0:T(8,128)(2,1)S(1)}, bf16[2,512,128]{2,1,0:T(8,128)(2,1)S(1)}, u32[]{:S(2)}, u32[]{:S(2)}) %collective-permute-start.6) | collective-permute-done | bytes 262176 | tf_op jit(solution)/shard_map/ppermute | solution.py:270
  33.8 2.8 %collective-permute-done.7.refs_6_ = bf16[2,512,128]{2,1,0:T(8,128)(2,1)S(1)} collective-permute-done((bf16[2,512,128]{2,1,0:T(8,128)(2,1)S(1)}, bf16[2,512,128]{2,1,0:T(8,128)(2,1)S(1)}, u32[]{:S(2)}, u32[]{:S(2)}) %collective-permute-start.7) | collective-permute-done | bytes 262176 | tf_op jit(solution)/shard_map/ppermute | solution.py:270
  36.6 14.8 %shard_map.123 = (bf16[512,128]{1,0:T(8,128)(2,1)S(1)}, bf16[512,128]{1,0:T(8,128)(2,1)S(1)}, bf16[512,128]{1,0:T(8,128)(2,1)S(1)}, bf16[512,128]{1,0:T(8,128)(2...) custom-call(bf16[2,512,128]{2,1,0:T(8,128)(2,1)S(1)} %get-tuple-elem, ...), custom_call_target="tpu_custom_call" | custom-call | flops 5368709120 | bytes 4194304 | tf_op jit(solution)/shard_map/pallas_call | solution.py:51
  51.4 2.3 collective-permute-start.12
  62.6 5.2 %collective-permute-done.14.refs_3_ = bf16[512,128]{1,0:T(8,128)(2,1)S(1)} collective-permute-done((bf16[512,128]{1,0:T(8,128)(2,1)S(1)}, bf16[512,128]{1,0:T(8,128)(2,1)S(1)}, u32[]{:S(2)}, u32[]{:S(2)}) %collective-permute-start.14) | collective-permute-done | bytes 131104 | tf_op jit(solution)/shard_map/ppermute | solution.py:270
  70.7 3.6 %collective-permute-start.34 = (bf16[512,128]{1,0:T(8,128)(2,1)S(1)}, bf16[512,128]{1,0:T(8,128)(2,1)S(1)}, u32[]{:S(2)}, u32[]{:S(2)}) collective-permute-start(bf16[512,128]{1,0:T(8,128)(2,1)S(1)} %get-tuple-element.61.refs_4_), channel_id=1, source_target_pairs={{0,4},{2,6},{4,0},{6,2},{1,5},{3,7},{5,1},{7,3},{8,12},{10,14},{12... | collective-permute-start | bytes 393224 | tf_op jit(solution)/shard_map/ppermute | solution.py:270
  76.4 19.3 %collective-permute-done.34.refs_6_ = bf16[512,128]{1,0:T(8,128)(2,1)S(1)} collective-permute-done((bf16[512,128]{1,0:T(8,128)(2,1)S(1)}, bf16[512,128]{1,0:T(8,128)(2,1)S(1)}, u32[]{:S(2)}, u32[]{:S(2)}) %collective-permute-start.34) | collective-permute-done | bytes 131104 | tf_op jit(solution)/shard_map/ppermute | solution.py:270
  96.7 4.6 %collective-permute-start.47 = (bf16[512,128]{1,0:T(8,128)(2,1)S(1)}, bf16[512,128]{1,0:T(8,128)(2,1)S(1)}, u32[]{:S(2)}, u32[]{:S(2)}) collective-permute-start(bf16[512,128]{1,0:T(8,128)(2,1)S(1)} %shard_map.124.refs_8_.refs_4_), channel_id=1, source_target_pairs={{0,4},{2,6},{4,0},{6,2},{1,5},{3,7},{5,1},{7,3},{8,12},{10,14},{12... | collective-permute-start | bytes 393224 | tf_op jit(solution)/shard_map/ppermute | solution.py:270
  101.5 2.8 %collective-permute-done.47.refs_6_ = bf16[512,128]{1,0:T(8,128)(2,1)S(1)} collective-permute-done((bf16[512,128]{1,0:T(8,128)(2,1)S(1)}, bf16[512,128]{1,0:T(8,128)(2,1)S(1)}, u32[]{:S(2)}, u32[]{:S(2)}) %collective-permute-start.47) | collective-permute-done | bytes 131104 | tf_op jit(solution)/shard_map/ppermute | solution.py:270
  104.3 17.0 %collective-permute-start.29 = (bf16[2,128,512]{2,1,0:T(8,128)(2,1)S(1)}, bf16[2,128,512]{2,1,0:T(8,128)(2,1)S(1)}, u32[]{:S(2)}, u32[]{:S(2)}) collective-permute-start(bf16[2,128,512]{2,1,0:T(8,128)(2,1)S(1)} %pad_maximum_fusion.5), channel_id=1, source_target_pairs={{0,6},{2,0},{4,2},{6,4},{1,7},{3,1},{5,3},{7,5},{8,14},{10,8},{12,... | collective-permute-start | bytes 786440 | tf_op jit(solution)/shard_map/ppermute | solution.py:270
  121.2 2.4 collective-permute-start.28
  123.6 2.8 %collective-permute-done.29 = bf16[2,128,512]{2,1,0:T(8,128)(2,1)S(1)} collective-permute-done((bf16[2,128,512]{2,1,0:T(8,128)(2,1)S(1)}, bf16[2,128,512]{2,1,0:T(8,128)(2,1)S(1)}, u32[]{:S(2)}, u32[]{:S(2)}) %collective-permute-start.29) | collective-permute-done | bytes 262176 | tf_op jit(solution)/shard_map/ppermute | solution.py:270
  126.5 4.3 %collective-permute-done.28 = bf16[2,128,512]{2,1,0:T(8,128)(2,1)S(1)} collective-permute-done((bf16[2,128,512]{2,1,0:T(8,128)(2,1)S(1)}, bf16[2,128,512]{2,1,0:T(8,128)(2,1)S(1)}, u32[]{:S(2)}, u32[]{:S(2)}) %collective-permute-start.28) | collective-permute-done | bytes 262176 | tf_op jit(solution)/shard_map/ppermute | solution.py:270
  132.7 2.2 collective-permute-start.32
  139.7 41.2 %collective-permute-done.30.refs_1_ = bf16[1024,512]{1,0:T(8,128)(2,1)S(1)} collective-permute-done((bf16[1024,512]{1,0:T(8,128)(2,1)S(1)}, bf16[1024,512]{1,0:T(8,128)(2,1)S(1)}, u32[]{:S(2)}, u32[]{:S(2)}) %collective-permute-start.30) | collective-permute-done | bytes 1048608 | tf_op jit(solution)/shard_map/ppermute | solution.py:270
  184.6 4.0 %collective-permute-done.15.refs_1_ = bf16[6,128,128]{2,1,0:T(8,128)(2,1)S(1)} collective-permute-done((bf16[6,128,128]{2,1,0:T(8,128)(2,1)S(1)}, bf16[6,128,128]{2,1,0:T(8,128)(2,1)S(1)}, u32[]{:S(2)}, u32[]{:S(2)}) %collective-permute-start.15) | collective-permute-done | bytes 196640 | tf_op jit(solution)/shard_map/ppermute | solution.py:270
  195.1 2.1 collective-permute-start.54
  198.7 4.6 %collective-permute-done.53.refs_1_ = bf16[128,512]{1,0:T(8,128)(2,1)S(1)} collective-permute-done((bf16[128,512]{1,0:T(8,128)(2,1)S(1)}, bf16[128,512]{1,0:T(8,128)(2,1)S(1)}, u32[]{:S(2)}, u32[]{:S(2)}) %collective-permute-start.53) | collective-permute-done | bytes 131104 | tf_op jit(solution)/shard_map/ppermute | solution.py:270
  204.1 5.1 %collective-permute-done.55.refs_3_ = bf16[128,512]{1,0:T(8,128)(2,1)S(1)} collective-permute-done((bf16[128,512]{1,0:T(8,128)(2,1)S(1)}, bf16[128,512]{1,0:T(8,128)(2,1)S(1)}, u32[]{:S(2)}, u32[]{:S(2)}) %collective-permute-start.55) | collective-permute-done | bytes 131104 | tf_op jit(solution)/shard_map/ppermute | solution.py:270
  209.2 6.3 %collective-permute-done.43.refs_1_ = bf16[512,128]{1,0:T(8,128)(2,1)S(1)} collective-permute-done((bf16[512,128]{1,0:T(8,128)(2,1)S(1)}, bf16[512,128]{1,0:T(8,128)(2,1)S(1)}, u32[]{:S(2)}, u32[]{:S(2)}) %collective-permute-start.43) | collective-permute-done | bytes 131104 | tf_op jit(solution)/shard_map/ppermute | solution.py:270
  215.7 6.3 %collective-permute-done.44.refs_2_ = bf16[512,128]{1,0:T(8,128)(2,1)S(1)} collective-permute-done((bf16[512,128]{1,0:T(8,128)(2,1)S(1)}, bf16[512,128]{1,0:T(8,128)(2,1)S(1)}, u32[]{:S(2)}, u32[]{:S(2)}) %collective-permute-start.44) | collective-permute-done | bytes 131104 | tf_op jit(solution)/shard_map/ppermute | solution.py:270
  223.3 3.6 %collective-permute-done.45.refs_3_ = bf16[512,128]{1,0:T(8,128)(2,1)S(1)} collective-permute-done((bf16[512,128]{1,0:T(8,128)(2,1)S(1)}, bf16[512,128]{1,0:T(8,128)(2,1)S(1)}, u32[]{:S(2)}, u32[]{:S(2)}) %collective-permute-start.45) | collective-permute-done | bytes 131104 | tf_op jit(solution)/shard_map/ppermute | solution.py:270
  226.9 6.7 %collective-permute-done.56.refs_1_ = bf16[512,128]{1,0:T(8,128)(2,1)S(1)} collective-permute-done((bf16[512,128]{1,0:T(8,128)(2,1)S(1)}, bf16[512,128]{1,0:T(8,128)(2,1)S(1)}, u32[]{:S(2)}, u32[]{:S(2)}) %collective-permute-start.56) | collective-permute-done | bytes 131104 | tf_op jit(solution)/shard_map/ppermute | solution.py:270
  234.5 5.6 %collective-permute-done.57.refs_2_ = bf16[512,128]{1,0:T(8,128)(2,1)S(1)} collective-permute-done((bf16[512,128]{1,0:T(8,128)(2,1)S(1)}, bf16[512,128]{1,0:T(8,128)(2,1)S(1)}, u32[]{:S(2)}, u32[]{:S(2)}) %collective-permute-start.57) | collective-permute-done | bytes 131104 | tf_op jit(solution)/shard_map/ppermute | solution.py:270
  240.1 2.9 %collective-permute-start.58 = (bf16[512,128]{1,0:T(8,128)(2,1)S(1)}, bf16[512,128]{1,0:T(8,128)(2,1)S(1)}, u32[]{:S(2)}, u32[]{:S(2)}) collective-permute-start(bf16[512,128]{1,0:T(8,128)(2,1)S(1)} %shard_map.133.refs_0_), channel_id=1, source_target_pairs={{0,96},{32,0},{64,32},{96,64},{1,97},{33,1},{65,33},{97,65},{2,98}... | collective-permute-start | bytes 393224 | tf_op jit(solution)/shard_map/ppermute | solution.py:270
  243.0 2.9 %shard_map.126 = bf16[128,2048]{1,0:T(8,128)(2,1)} custom-call(bf16[6,128,128]{2,1,0:T(8,128)(2,1)S(1)} %get-tuple-element.55.refs_0_, bf16[6,128,128]{2,1,0:T(8,128)(2,1)S(1)} %collective-permute-done.15.refs_1_, bf16[6,128,128]{2,1,0:T(8,128)(2,1)S(1)} %collective-permute-done.16.refs_2_, bf16[6,128,128]{2,1,0:T(8,128)(2,1)S(1)} %collective-permute-done.17.refs_3_, ...), custom_call_target="tpu_custom_call" | custom-call | bytes 1048576 | tf_op jit(solution)/shard_map/pallas_call | solution.py:51
  248.2 3.8 %shard_map.127 = bf16[128,4096]{1,0:T(8,128)(2,1)} custom-call(bf16[6,128,128]{2,1,0:T(8,128)(2,1)S(1)} %get-tuple-element.55.refs_0_, bf16[6,128,128]{2,1,0:T(8,128)(2,1)S(1)} %collective-permute-done.15.refs_1_, bf16[6,128,128]{2,1,0:T(8,128)(2,1)S(1)} %collective-permute-done.16.refs_2_, bf16[6,128,128]{2,1,0:T(8,128)(2,1)S(1)} %collective-permute-done.17.refs_3_, ...), custom_call_target="tpu_custom_call" | custom-call | flops 1073741824 | bytes 9437184 | tf_op jit(solution)/shard_map/pallas_call | solution.py:51
  (141 shorter events, 55.6 us)
Async XLA Ops:
  6.0 21.9 %collective-permute-start = (bf16[2,512,128]{2,1,0:T(8,128)(2,1)S(1)}, bf16[2,512,128]{2,1,0:T(8,128)(2,1)S(1)}, u32[]{:S(2)}, u32[]{:S(2)}) collective-permute-start(bf16[2,512,128]{2,1,0:T(8,128)(2,1)S(1)} %get-tuple-element.34), channel_id=1, source_target_pairs={{0,32},{32,64},{64,96},{96,0},{1,33},{33,65},{65,97},{97,1},{2,34}... | collective-permute-start | bytes 786440 | tf_op jit(solution)/shard_map/ppermute | solution.py:270
  12.0 10.9 %collective-permute-start.4 = (bf16[3,128,128]{2,1,0:T(8,128)(2,1)S(1)}, bf16[3,128,128]{2,1,0:T(8,128)(2,1)S(1)}, u32[]{:S(2)}, u32[]{:S(2)}) collective-permute-start(bf16[3,128,128]{2,1,0:T(8,128)(2,1)S(1)} %get-tuple-element.39), channel_id=1, source_target_pairs={{0,64},{32,96},{64,0},{96,32},{1,65},{33,97},{65,1},{97,33},{2,66}... | collective-permute-start | bytes 294920 | tf_op jit(solution)/shard_map/ppermute | solution.py:270
  13.7 9.7 %collective-permute-start.5 = (bf16[3,128,128]{2,1,0:T(8,128)(2,1)S(1)}, bf16[3,128,128]{2,1,0:T(8,128)(2,1)S(1)}, u32[]{:S(2)}, u32[]{:S(2)}) collective-permute-start(bf16[3,128,128]{2,1,0:T(8,128)(2,1)S(1)} %get-tuple-element.40), channel_id=1, source_target_pairs={{0,96},{32,0},{64,32},{96,64},{1,97},{33,1},{65,33},{97,65},{2,98}... | collective-permute-start | bytes 294920 | tf_op jit(solution)/shard_map/ppermute | solution.py:270
  16.3 13.0 %collective-permute-start.1 = (bf16[2,512,128]{2,1,0:T(8,128)(2,1)S(1)}, bf16[2,512,128]{2,1,0:T(8,128)(2,1)S(1)}, u32[]{:S(2)}, u32[]{:S(2)}) collective-permute-start(bf16[2,512,128]{2,1,0:T(8,128)(2,1)S(1)} %get-tuple-element.35), channel_id=1, source_target_pairs={{0,64},{32,96},{64,0},{96,32},{1,65},{33,97},{65,1},{97,33},{2,66}... | collective-permute-start | bytes 786440 | tf_op jit(solution)/shard_map/ppermute | solution.py:270
  18.5 11.5 %collective-permute-start.2 = (bf16[2,512,128]{2,1,0:T(8,128)(2,1)S(1)}, bf16[2,512,128]{2,1,0:T(8,128)(2,1)S(1)}, u32[]{:S(2)}, u32[]{:S(2)}) collective-permute-start(bf16[2,512,128]{2,1,0:T(8,128)(2,1)S(1)} %get-tuple-element.36), channel_id=1, source_target_pairs={{0,96},{32,0},{64,32},{96,64},{1,97},{33,1},{65,33},{97,65},{2,98}... | collective-permute-start | bytes 786440 | tf_op jit(solution)/shard_map/ppermute | solution.py:270
  23.5 10.3 %collective-permute-start.6 = (bf16[2,512,128]{2,1,0:T(8,128)(2,1)S(1)}, bf16[2,512,128]{2,1,0:T(8,128)(2,1)S(1)}, u32[]{:S(2)}, u32[]{:S(2)}) collective-permute-start(bf16[2,512,128]{2,1,0:T(8,128)(2,1)S(1)} %get-tuple-element.41.refs_4_), channel_id=1, source_target_pairs={{0,8},{8,16},{16,24},{24,0},{1,9},{9,17},{17,25},{25,1},{2,10},{10... | collective-permute-start | bytes 786440 | tf_op jit(solution)/shard_map/ppermute | solution.py:270
  25.1 11.5 %collective-permute-start.7 = (bf16[2,512,128]{2,1,0:T(8,128)(2,1)S(1)}, bf16[2,512,128]{2,1,0:T(8,128)(2,1)S(1)}, u32[]{:S(2)}, u32[]{:S(2)}) collective-permute-start(bf16[2,512,128]{2,1,0:T(8,128)(2,1)S(1)} %get-tuple-element.41.refs_4_), channel_id=1, source_target_pairs={{0,16},{8,24},{16,0},{24,8},{1,17},{9,25},{17,1},{25,9},{2,18},{10... | collective-permute-start | bytes 786440 | tf_op jit(solution)/shard_map/ppermute | solution.py:270
  29.3 45.1 %collective-permute-start.26 = (bf16[4,128,512]{2,1,0:T(8,128)(2,1)S(1)}, bf16[4,128,512]{2,1,0:T(8,128)(2,1)S(1)}, u32[]{:S(2)}, u32[]{:S(2)}) collective-permute-start(bf16[4,128,512]{2,1,0:T(8,128)(2,1)S(1)} %get-tuple-element.60), channel_id=1, source_target_pairs={{0,1},{1,0},{2,3},{3,2},{4,5},{5,4},{6,7},{7,6},{8,9},{9,8},{10,11... | collective-permute-start | bytes 1572872 | tf_op jit(solution)/shard_map/ppermute | solution.py:270
  54.9 13.5 %collective-permute-start.9 = (bf16[512,128]{1,0:T(8,128)(2,1)S(1)}, bf16[512,128]{1,0:T(8,128)(2,1)S(1)}, u32[]{:S(2)}, u32[]{:S(2)}) collective-permute-start(bf16[512,128]{1,0:T(8,128)(2,1)S(1)} %get-tuple-element.43), channel_id=1, source_target_pairs={{0,24},{8,0},{16,8},{24,16},{1,25},{9,1},{17,9},{25,17},{2,26},{10... | collective-permute-start | bytes 393224 | tf_op jit(solution)/shard_map/ppermute | solution.py:270
  56.2 12.2 %collective-permute-start.10 = (bf16[512,128]{1,0:T(8,128)(2,1)S(1)}, bf16[512,128]{1,0:T(8,128)(2,1)S(1)}, u32[]{:S(2)}, u32[]{:S(2)}) collective-permute-start(bf16[512,128]{1,0:T(8,128)(2,1)S(1)} %get-tuple-element.44), channel_id=1, source_target_pairs={{0,16},{8,24},{16,0},{24,8},{1,17},{9,25},{17,1},{25,9},{2,18},{10... | collective-permute-start | bytes 393224 | tf_op jit(solution)/shard_map/ppermute | solution.py:270
  57.7 10.7 %collective-permute-start.11 = (bf16[512,128]{1,0:T(8,128)(2,1)S(1)}, bf16[512,128]{1,0:T(8,128)(2,1)S(1)}, u32[]{:S(2)}, u32[]{:S(2)}) collective-permute-start(bf16[512,128]{1,0:T(8,128)(2,1)S(1)} %get-tuple-element.45), channel_id=1, source_target_pairs={{0,8},{8,16},{16,24},{24,0},{1,9},{9,17},{17,25},{25,1},{2,10},{10... | collective-permute-start | bytes 393224 | tf_op jit(solution)/shard_map/ppermute | solution.py:270
  67.8 67.1 %collective-permute-start.20 = (bf16[2,512,512]{2,1,0:T(8,128)(2,1)S(1)}, bf16[2,512,512]{2,1,0:T(8,128)(2,1)S(1)}, u32[]{:S(2)}, u32[]{:S(2)}) collective-permute-start(bf16[2,512,512]{2,1,0:T(8,128)(2,1)S(1)} %pad_maximum_fusion.refs_4_), channel_id=1, source_target_pairs={{0,6},{2,0},{4,2},{6,4},{1,7},{3,1},{5,3},{7,5},{8,14},{10,8},{12,... | collective-permute-start | bytes 3145736 | tf_op jit(solution)/shard_map/ppermute | solution.py:270
  70.7 25.1 %collective-permute-start.34 = (bf16[512,128]{1,0:T(8,128)(2,1)S(1)}, bf16[512,128]{1,0:T(8,128)(2,1)S(1)}, u32[]{:S(2)}, u32[]{:S(2)}) collective-permute-start(bf16[512,128]{1,0:T(8,128)(2,1)S(1)} %get-tuple-element.61.refs_4_), channel_id=1, source_target_pairs={{0,4},{2,6},{4,0},{6,2},{1,5},{3,7},{5,1},{7,3},{8,12},{10,14},{12... | collective-permute-start | bytes 393224 | tf_op jit(solution)/shard_map/ppermute | solution.py:270
  74.3 22.4 %collective-permute-start.35 = (bf16[512,128]{1,0:T(8,128)(2,1)S(1)}, bf16[512,128]{1,0:T(8,128)(2,1)S(1)}, u32[]{:S(2)}, u32[]{:S(2)}) collective-permute-start(bf16[512,128]{1,0:T(8,128)(2,1)S(1)} %get-tuple-element.61.refs_4_), channel_id=1, source_target_pairs={{0,6},{2,0},{4,2},{6,4},{1,7},{3,1},{5,3},{7,5},{8,14},{10,8},{12,... | collective-permute-start | bytes 393224 | tf_op jit(solution)/shard_map/ppermute | solution.py:270
  74.4 26.9 %collective-permute-start.36 = (bf16[512,128]{1,0:T(8,128)(2,1)S(1)}, bf16[512,128]{1,0:T(8,128)(2,1)S(1)}, u32[]{:S(2)}, u32[]{:S(2)}) collective-permute-start(bf16[512,128]{1,0:T(8,128)(2,1)S(1)} %get-tuple-element.61.refs_4_), channel_id=1, source_target_pairs={{0,1},{1,0},{2,3},{3,2},{4,5},{5,4},{6,7},{7,6},{8,9},{9,8},{10,11... | collective-permute-start | bytes 393224 | tf_op jit(solution)/shard_map/ppermute | solution.py:270
  75.0 26.3 %collective-permute-start.46 = (bf16[512,128]{1,0:T(8,128)(2,1)S(1)}, bf16[512,128]{1,0:T(8,128)(2,1)S(1)}, u32[]{:S(2)}, u32[]{:S(2)}) collective-permute-start(bf16[512,128]{1,0:T(8,128)(2,1)S(1)} %shard_map.124.refs_8_.refs_4_), channel_id=1, source_target_pairs={{0,2},{2,4},{4,6},{6,0},{1,3},{3,5},{5,7},{7,1},{8,10},{10,12},{12... | collective-permute-start | bytes 393224 | tf_op jit(solution)/shard_map/ppermute | solution.py:270
  95.7 40.7 %collective-permute-start.18 = (bf16[2,512,512]{2,1,0:T(8,128)(2,1)S(1)}, bf16[2,512,512]{2,1,0:T(8,128)(2,1)S(1)}, u32[]{:S(2)}, u32[]{:S(2)}) collective-permute-start(bf16[2,512,512]{2,1,0:T(8,128)(2,1)S(1)} %pad_maximum_fusion.refs_4_), channel_id=1, source_target_pairs={{0,2},{2,4},{4,6},{6,0},{1,3},{3,5},{5,7},{7,1},{8,10},{10,12},{12... | collective-permute-start | bytes 3145736 | tf_op jit(solution)/shard_map/ppermute | solution.py:270
  101.3 19.9 %collective-permute-start.48 = (bf16[512,128]{1,0:T(8,128)(2,1)S(1)}, bf16[512,128]{1,0:T(8,128)(2,1)S(1)}, u32[]{:S(2)}, u32[]{:S(2)}) collective-permute-start(bf16[512,128]{1,0:T(8,128)(2,1)S(1)} %shard_map.124.refs_8_.refs_4_), channel_id=1, source_target_pairs={{0,6},{2,0},{4,2},{6,4},{1,7},{3,1},{5,3},{7,5},{8,14},{10,8},{12,... | collective-permute-start | bytes 393224 | tf_op jit(solution)/shard_map/ppermute | solution.py:270
  101.3 22.3 %collective-permute-start.49 = (bf16[512,128]{1,0:T(8,128)(2,1)S(1)}, bf16[512,128]{1,0:T(8,128)(2,1)S(1)}, u32[]{:S(2)}, u32[]{:S(2)}) collective-permute-start(bf16[512,128]{1,0:T(8,128)(2,1)S(1)} %shard_map.124.refs_8_.refs_4_), channel_id=1, source_target_pairs={{0,1},{1,0},{2,3},{3,2},{4,5},{5,4},{6,7},{7,6},{8,9},{9,8},{10,11... | collective-permute-start | bytes 393224 | tf_op jit(solution)/shard_map/ppermute | solution.py:270
  104.3 22.2 %collective-permute-start.29 = (bf16[2,128,512]{2,1,0:T(8,128)(2,1)S(1)}, bf16[2,128,512]{2,1,0:T(8,128)(2,1)S(1)}, u32[]{:S(2)}, u32[]{:S(2)}) collective-permute-start(bf16[2,128,512]{2,1,0:T(8,128)(2,1)S(1)} %pad_maximum_fusion.5), channel_id=1, source_target_pairs={{0,6},{2,0},{4,2},{6,4},{1,7},{3,1},{5,3},{7,5},{8,14},{10,8},{12,... | collective-permute-start | bytes 786440 | tf_op jit(solution)/shard_map/ppermute | solution.py:270
  121.2 9.5 %collective-permute-start.28 = (bf16[2,128,512]{2,1,0:T(8,128)(2,1)S(1)}, bf16[2,128,512]{2,1,0:T(8,128)(2,1)S(1)}, u32[]{:S(2)}, u32[]{:S(2)}) collective-permute-start(bf16[2,128,512]{2,1,0:T(8,128)(2,1)S(1)} %pad_maximum_fusion.4), channel_id=1, source_target_pairs={{0,4},{2,6},{4,0},{6,2},{1,5},{3,7},{5,1},{7,3},{8,12},{10,14},{12... | collective-permute-start | bytes 786440 | tf_op jit(solution)/shard_map/ppermute | solution.py:270
  131.5 49.3 %collective-permute-start.30 = (bf16[1024,512]{1,0:T(8,128)(2,1)S(1)}, bf16[1024,512]{1,0:T(8,128)(2,1)S(1)}, u32[]{:S(2)}, u32[]{:S(2)}) collective-permute-start(bf16[1024,512]{1,0:T(8,128)(2,1)S(1)} %bitcast.23), channel_id=1, source_target_pairs={{0,32},{32,64},{64,96},{96,0},{1,33},{33,65},{65,97},{97,1},{2,34}... | collective-permute-start | bytes 3145736 | tf_op jit(solution)/shard_map/ppermute | solution.py:270
  132.1 48.8 %collective-permute-start.31 = (bf16[1024,512]{1,0:T(8,128)(2,1)S(1)}, bf16[1024,512]{1,0:T(8,128)(2,1)S(1)}, u32[]{:S(2)}, u32[]{:S(2)}) collective-permute-start(bf16[1024,512]{1,0:T(8,128)(2,1)S(1)} %bitcast.24), channel_id=1, source_target_pairs={{0,64},{32,96},{64,0},{96,32},{1,65},{33,97},{65,1},{97,33},{2,66}... | collective-permute-start | bytes 3145736 | tf_op jit(solution)/shard_map/ppermute | solution.py:270
  132.7 48.7 %collective-permute-start.32 = (bf16[1024,512]{1,0:T(8,128)(2,1)S(1)}, bf16[1024,512]{1,0:T(8,128)(2,1)S(1)}, u32[]{:S(2)}, u32[]{:S(2)}) collective-permute-start(bf16[1024,512]{1,0:T(8,128)(2,1)S(1)} %bitcast.25), channel_id=1, source_target_pairs={{0,96},{32,0},{64,32},{96,64},{1,97},{33,1},{65,33},{97,65},{2,98}... | collective-permute-start | bytes 3145736 | tf_op jit(solution)/shard_map/ppermute | solution.py:270
  137.6 56.5 %collective-permute-start.21 = (bf16[512,512]{1,0:T(8,128)(2,1)S(1)}, bf16[512,512]{1,0:T(8,128)(2,1)S(1)}, u32[]{:S(2)}, u32[]{:S(2)}) collective-permute-start(bf16[512,512]{1,0:T(8,128)(2,1)S(1)} %slice_bitcast_fusion), channel_id=1, source_target_pairs={{0,6},{2,0},{4,2},{6,4},{1,7},{3,1},{5,3},{7,5},{8,14},{10,8},{12,... | collective-permute-start | bytes 1572872 | tf_op jit(solution)/shard_map/ppermute | solution.py:270
  138.2 56.9 %collective-permute-start.19 = (bf16[512,512]{1,0:T(8,128)(2,1)S(1)}, bf16[512,512]{1,0:T(8,128)(2,1)S(1)}, u32[]{:S(2)}, u32[]{:S(2)}) collective-permute-start(bf16[512,512]{1,0:T(8,128)(2,1)S(1)} %slice_bitcast_fusion.1), channel_id=1, source_target_pairs={{0,2},{2,4},{4,6},{6,0},{1,3},{3,5},{5,7},{7,1},{8,10},{10,12},{12... | collective-permute-start | bytes 1572872 | tf_op jit(solution)/shard_map/ppermute | solution.py:270
  180.9 9.3 %collective-permute-start.16 = (bf16[6,128,128]{2,1,0:T(8,128)(2,1)S(1)}, bf16[6,128,128]{2,1,0:T(8,128)(2,1)S(1)}, u32[]{:S(2)}, u32[]{:S(2)}) collective-permute-start(bf16[6,128,128]{2,1,0:T(8,128)(2,1)S(1)} %get-tuple-element.57), channel_id=1, source_target_pairs={{0,64},{32,96},{64,0},{96,32},{1,65},{33,97},{65,1},{97,33},{2,66}... | collective-permute-start | bytes 589832 | tf_op jit(solution)/shard_map/ppermute | solution.py:270
  181.5 11.6 %collective-permute-start.17 = (bf16[6,128,128]{2,1,0:T(8,128)(2,1)S(1)}, bf16[6,128,128]{2,1,0:T(8,128)(2,1)S(1)}, u32[]{:S(2)}, u32[]{:S(2)}) collective-permute-start(bf16[6,128,128]{2,1,0:T(8,128)(2,1)S(1)} %get-tuple-element.58), channel_id=1, source_target_pairs={{0,32},{32,64},{64,96},{96,0},{1,33},{33,65},{65,97},{97,1},{2,34}... | collective-permute-start | bytes 589832 | tf_op jit(solution)/shard_map/ppermute | solution.py:270
  197.3 50.9 %collective-permute-start.22 = (bf16[2,512,512]{2,1,0:T(8,128)(2,1)S(1)}, bf16[2,512,512]{2,1,0:T(8,128)(2,1)S(1)}, u32[]{:S(2)}, u32[]{:S(2)}) collective-permute-start(bf16[2,512,512]{2,1,0:T(8,128)(2,1)S(1)} %pad_maximum_fusion.refs_4_), channel_id=1, source_target_pairs={{0,1},{1,0},{2,3},{3,2},{4,5},{5,4},{6,7},{7,6},{8,9},{9,8},{10,11... | collective-permute-start | bytes 3145736 | tf_op jit(solution)/shard_map/ppermute | solution.py:270
  197.4 50.8 %collective-permute-start.23 = (bf16[2,512,512]{2,1,0:T(8,128)(2,1)S(1)}, bf16[2,512,512]{2,1,0:T(8,128)(2,1)S(1)}, u32[]{:S(2)}, u32[]{:S(2)}) collective-permute-start(bf16[2,512,512]{2,1,0:T(8,128)(2,1)S(1)} %collective-permute-done.18.refs_5_), channel_id=1, source_target_pairs={{0,1},{1,0},{2,3},{3,2},{4,5},{5,4},{6,7},{7,6},{8,9},{9,8},{10,11... | collective-permute-start | bytes 3145736 | tf_op jit(solution)/shard_map/ppermute | solution.py:270
  198.7 49.4 %collective-permute-start.25 = (bf16[2,512,512]{2,1,0:T(8,128)(2,1)S(1)}, bf16[2,512,512]{2,1,0:T(8,128)(2,1)S(1)}, u32[]{:S(2)}, u32[]{:S(2)}) collective-permute-start(bf16[2,512,512]{2,1,0:T(8,128)(2,1)S(1)} %collective-permute-done.20.refs_7_), channel_id=1, source_target_pairs={{0,1},{1,0},{2,3},{3,2},{4,5},{5,4},{6,7},{7,6},{8,9},{9,8},{10,11... | collective-permute-start | bytes 3145736 | tf_op jit(solution)/shard_map/ppermute | solution.py:270
  203.3 44.9 %collective-permute-start.24 = (bf16[2,512,512]{2,1,0:T(8,128)(2,1)S(1)}, bf16[2,512,512]{2,1,0:T(8,128)(2,1)S(1)}, u32[]{:S(2)}, u32[]{:S(2)}) collective-permute-start(bf16[2,512,512]{2,1,0:T(8,128)(2,1)S(1)} %pad_maximum_fusion.1.refs_6_), channel_id=1, source_target_pairs={{0,1},{1,0},{2,3},{3,2},{4,5},{5,4},{6,7},{7,6},{8,9},{9,8},{10,11... | collective-permute-start | bytes 3145736 | tf_op jit(solution)/shard_map/ppermute | solution.py:270
  (37 other events, 296.3 us)
where the time goes:
time: 252 us
  waiting for transfers between devices  139 us (55%)
  starting transfers between devices  77.4 us (31%)
  Pallas kernels  29 us (12%)
  local copies, waits for them, and re-layouts  4.45 us (2%)
    ppermute x59, waiting for transfers between devices, shift(): return lax.ppermute(array, name, [(i, (i + by) % n) for i in range(n)])  139 us
    ppermute x59, starting transfers between devices, shift(): return lax.ppermute(array, name, [(i, (i + by) % n) for i in range(n)])  77.4 us
    pallas_call x15, Pallas kernels, call(): pl.pallas_call(body, out_shape=[jax.ShapeDtypeStruct(s, d) for s, d in ou...  29 us
  transfers between devices with their start and end apart: 59, of which 31 were waited for; matrix products, arithmetic and copies ran while one was open for 0% of the time, Pallas kernels for 9%

commit v1 on v0

--- a/solution.py
+++ b/solution.py
@@ -25,7 +25,7 @@
 BF = jnp.bfloat16
 SCALE = HEAD_DIM**-0.5
 EXP2_SCALE = SCALE * math.log2(math.e)
-CHUNK = 512
+CHUNK = 1024
 
 
 def rope_tables():
@@ -217,27 +217,30 @@
             out[:, cols] = backward_rotate(g, u, qg_ref[...], cos, sin).astype(BF)
 
 
-def cut_input_body(in_ref, own, sib):
-    y, c = axis("y"), axis("c")
-    for s in range(4):
-        there = cyc(y + s)
-        own[s] = in_ref[:, span(2 * there + c, GROUP_COLS)]
-        sib[s] = in_ref[:, span(2 * there + 1 - c, GROUP_COLS)]
+def cut_input_body(in_ref, *outs):
+    for s in range(4):
+        outs[s][...] = in_ref[:, span(cyc(axis("y") + s), 1024)]
 
 
 def weight_body(*refs):
-    inputs, own, sib = refs[0:4], refs[4:8], refs[8:12]
-    out, right = refs[12:]
+    inputs, kv = refs[0:4], refs[4:8]
+    own, sib, right = refs[8:]
     for b in range(4):
         for s in range(4):
-            for p, kv in ((0, own), (1, sib)):
-                rows = pl.ds(b * 1024 + (2 * s + p) * TOK, TOK)
-                right[rows, :] = kv[s][pl.ds(b * TOK, TOK), :]
-    total = None
-    for b in range(4):
-        part = dg(right[pl.ds(b * 1024, 1024), :], inputs[b][...], 0, 0)
-        total = part if total is None else total + part
-    out[...] = total.astype(BF)
+            rows = pl.ds(b * 512 + s * TOK, TOK)
+            right[rows, :] = kv[s][pl.ds(b * TOK, TOK), :]
+    core = axis("c")
+    for out, which in ((sib, 1 - core), (own, core)):
+        total = None
+        for b in range(4):
+            left = right[pl.ds(b * 512, 512), :]
+            part = dg(left, inputs[b][:, span(which, GROUP_COLS)], 0, 0)
+            total = part if total is None else total + part
+        out[...] = total.astype(out.dtype)
+
+
+def pair_sum_body(own, sib, out):
+    out[...] = (own[...] + sib[...].astype(F32)).astype(BF)
 
 
 def sum_weight_body(*refs):
@@ -302,13 +305,9 @@
     kv_here, raw_keys = call(join_kv_body, [((2, 512, 128), BF), square], kv_pieces)
     kv_parts = exchange([kv_here] * 4, "x")
 
-    in_own, in_sib = call(cut_input_body, [((4, 128, 512), BF)] * 2, (layer_in,))
-    in_sib = shift(in_sib, "c", 1)
-    in_msgs = [None] + [jnp.stack([in_own[s], in_sib[s]]) for s in (1, 2, 3)]
-    in_parts = exchange(in_msgs, "y")
-    in_first = jnp.stack([in_own[0], in_sib[0]])
-    in_all = jnp.stack([in_first, *in_parts[1:]]).reshape(1024, 512)
-    inputs = exchange([in_all] * 4, "z")
+    cuts = call(cut_input_body, [((128, 1024), BF)] * 4, (layer_in,))
+    in_parts = exchange(cuts, "y")
+    inputs = exchange([jnp.concatenate(in_parts)] * 4, "z")
 
     weights = jnp.stack([key_weight, value_weight])
     w_prev = shift(weights, "y", 1)
@@ -324,7 +323,7 @@
         scratch=[pltpu.VMEM((LEN, 128), BF)] * 5 + [pltpu.VMEM((128, LEN), F32)] * 2,
         flops=5 * 2 * LEN * LEN * 128,
         nbytes=4 << 20,
-        limit=32,
+        limit=44,
     )
     dq_out, dk_out, dv_out = attended[:4], attended[4:8], attended[8:]
     dv_parts = exchange(dv_out, "x", -1)
@@ -332,7 +331,6 @@
 
     (v_sum,) = call(sum_v_body, [square], dv_parts)
     v_own = exchange([v_sum] * 4, "y")
-    v_sib = [shift(a, "c", 1) for a in v_own]
 
     k_sum, *token_grads = call(
         k_back_body,
@@ -340,30 +338,33 @@
         (*dk_parts, *dq_out, v_sum, raw_keys, kg, *tables),
     )
     k_own = exchange([k_sum] * 4, "y")
-    k_sib = [shift(a, "c", 1) for a in k_own]
     token_grads = exchange(token_grads, "z", -1)
 
     (grad_query,) = call(
         q_back_body, [((128, 2048), BF)], (*token_grads, queries, qg, *tables)
     )
 
-    def weight_chain(own, sib):
-        (part,) = call(
+    wide = (128, 512)
+
+    def weight_chain(kv):
+        own, sib = call(
             weight_body,
-            [((128, 512), BF)],
-            (*inputs, *own, *sib),
-            scratch=[pltpu.VMEM((4096, 128), BF)],
+            [(wide, F32), (wide, BF)],
+            (*inputs, *kv),
+            scratch=[pltpu.VMEM((2048, 128), BF)],
             flops=2 * 4096 * 512 * 128,
             limit=16,
         )
+        sib = shift(sib, "c", 1)
+        (part,) = call(pair_sum_body, [(wide, BF)], (own, sib))
         parts = exchange([part] * 4, "x")
         (total,) = call(sum_weight_body, [square], parts)
         blocks = exchange([total] * 4, "z")
         (out,) = call(place_weight_body, [((512, 512), F32)], blocks)
         return out
 
-    grad_value_weight = weight_chain(v_own, v_sib)
-    grad_key_weight = weight_chain(k_own, k_sib)
+    grad_value_weight = weight_chain(v_own)
+    grad_key_weight = weight_chain(k_own)
     (grad_in,) = call(
         input_grad_body,
         [((128, 4096), BF)],

time: 252 us -> 201 us (0.80)
  waiting for transfers between devices: 139 us -> 104 us
  starting transfers between devices: 77.4 us -> 61.5 us
    ppermute x59 -> x52, waiting for transfers between devices: 139 us -> 104 us  [shift(): return lax.ppermute(array, name, [(i, (i + by) % n) for i in range(n)])]
    ppermute x59 -> x52, starting transfers between devices: 77.4 us -> 61.5 us  [shift(): return lax.ppermute(array, name, [(i, (i + by) % n) for i in range(n)])]
    pallas_call x15 -> x17, Pallas kernels: 29 us -> 27.8 us  [call(): pl.pallas_call(body, out_shape=[jax.ShapeDtypeStruct(s, d) for s, d in ou...]
    unnamed x20 -> x23, local copies, waits for them, and re-layouts: 4.31 us -> 5.48 us
  transfers between devices with their start and end apart: 59 -> 52, of which waited for: 31 -> 25; matrix products, arithmetic and copies ran while one was open for 0% -> 0% of each run, Pallas kernels for 9% -> 11%
where the time goes in v1:
time: 201 us
  waiting for transfers between devices  104 us (52%)
  starting transfers between devices  61.5 us (31%)
  Pallas kernels  27.8 us (14%)
  local copies, waits for them, and re-layouts  5.57 us (3%)
    ppermute x52, waiting for transfers between devices, shift(): return lax.ppermute(array, name, [(i, (i + by) % n) for i in range(n)])  104 us
    ppermute x52, starting transfers between devices, shift(): return lax.ppermute(array, name, [(i, (i + by) % n) for i in range(n)])  61.5 us
    pallas_call x17, Pallas kernels, call(): pl.pallas_call(body, out_shape=[jax.ShapeDtypeStruct(s, d) for s, d in ou...  27.8 us
    unnamed x23, local copies, waits for them, and re-layouts  5.48 us
  transfers between devices with their start and end apart: 52, of which 25 were waited for; matrix products, arithmetic and copies ran while one was open for 0% of the time, Pallas kernels for 11%

profile of v1, /device:TPU:8, one launch (start us, length us, event | category | flops | bytes accessed | tf_op | source)
XLA Modules:
  0.0 200.8 jit_solution(8606212144905706504)
XLA Ops:
  13.7 2.5 %collective-permute-start.5 = (bf16[3,128,128]{2,1,0:T(8,128)(2,1)S(1)}, bf16[3,128,128]{2,1,0:T(8,128)(2,1)S(1)}, u32[]{:S(2)}, u32[]{:S(2)}) collective-permute-start(bf16[3,128,128]{2,1,0:T(8,128)(2,1)S(1)} %get-tuple-element.46), channel_id=1, source_target_pairs={{0,96},{32,0},{64,32},{96,64},{1,97},{33,1},{65,33},{97,65},{2,98}... | collective-permute-start | bytes 294920 | tf_op jit(solution)/shard_map/ppermute | solution.py:273
  16.3 2.2 %collective-permute-done.3.refs_1_ = bf16[3,128,128]{2,1,0:T(8,128)(2,1)S(1)} collective-permute-done((bf16[3,128,128]{2,1,0:T(8,128)(2,1)S(1)}, bf16[3,128,128]{2,1,0:T(8,128)(2,1)S(1)}, u32[]{:S(2)}, u32[]{:S(2)}) %collective-permute-start.3) | collective-permute-done | bytes 98336 | tf_op jit(solution)/shard_map/ppermute | solution.py:273
  18.5 2.9 %collective-permute-start.2 = (bf16[2,512,128]{2,1,0:T(8,128)(2,1)S(1)}, bf16[2,512,128]{2,1,0:T(8,128)(2,1)S(1)}, u32[]{:S(2)}, u32[]{:S(2)}) collective-permute-start(bf16[2,512,128]{2,1,0:T(8,128)(2,1)S(1)} %get-tuple-element.42), channel_id=1, source_target_pairs={{0,96},{32,0},{64,32},{96,64},{1,97},{33,1},{65,33},{97,65},{2,98}... | collective-permute-start | bytes 786440 | tf_op jit(solution)/shard_map/ppermute | solution.py:273
  25.1 2.7 %collective-permute-start.7 = (bf16[2,512,128]{2,1,0:T(8,128)(2,1)S(1)}, bf16[2,512,128]{2,1,0:T(8,128)(2,1)S(1)}, u32[]{:S(2)}, u32[]{:S(2)}) collective-permute-start(bf16[2,512,128]{2,1,0:T(8,128)(2,1)S(1)} %get-tuple-element.47.refs_4_), channel_id=1, source_target_pairs={{0,16},{8,24},{16,0},{24,8},{1,17},{9,25},{17,1},{25,9},{2,18},{10... | collective-permute-start | bytes 786440 | tf_op jit(solution)/shard_map/ppermute | solution.py:273
  33.8 2.4 %collective-permute-start.27 = (bf16[128,1024]{1,0:T(8,128)(2,1)S(1)}, bf16[128,1024]{1,0:T(8,128)(2,1)S(1)}, u32[]{:S(2)}, u32[]{:S(2)}) collective-permute-start(bf16[128,1024]{1,0:T(8,128)(2,1)S(1)} %get-tuple-element.67), channel_id=1, source_target_pairs={{0,4},{2,6},{4,0},{6,2},{1,5},{3,7},{5,1},{7,3},{8,12},{10,14},{12... | collective-permute-start | bytes 786440 | tf_op jit(solution)/shard_map/ppermute | solution.py:273
  37.4 13.6 %shard_map.123 = (bf16[512,128]{1,0:T(8,128)(2,1)S(1)}, bf16[512,128]{1,0:T(8,128)(2,1)S(1)}, bf16[512,128]{1,0:T(8,128)(2,1)S(1)}, bf16[512,128]{1,0:T(8,128)(2...) custom-call(bf16[2,512,128]{2,1,0:T(8,128)(2,1)S(1)} %get-tuple-elem, ...), custom_call_target="tpu_custom_call" | custom-call | flops 5368709120 | bytes 4194304 | tf_op jit(solution)/shard_map/pallas_call | solution.py:51
  53.7 7.7 %collective-permute-done.27 = bf16[128,1024]{1,0:T(8,128)(2,1)S(1)} collective-permute-done((bf16[128,1024]{1,0:T(8,128)(2,1)S(1)}, bf16[128,1024]{1,0:T(8,128)(2,1)S(1)}, u32[]{:S(2)}, u32[]{:S(2)}) %collective-permute-start.27) | collective-permute-done | bytes 262176 | tf_op jit(solution)/shard_map/ppermute | solution.py:273
  64.7 2.4 %collective-permute-start.12 = (bf16[512,128]{1,0:T(8,128)(2,1)S(1)}, bf16[512,128]{1,0:T(8,128)(2,1)S(1)}, u32[]{:S(2)}, u32[]{:S(2)}) collective-permute-start(bf16[512,128]{1,0:T(8,128)(2,1)S(1)} %get-tuple-element.57), channel_id=1, source_target_pairs={{0,24},{8,0},{16,8},{24,16},{1,25},{9,1},{17,9},{25,17},{2,26},{10... | collective-permute-start | bytes 393224 | tf_op jit(solution)/shard_map/ppermute | solution.py:273
  69.8 3.9 %collective-permute-done.13.refs_2_ = bf16[512,128]{1,0:T(8,128)(2,1)S(1)} collective-permute-done((bf16[512,128]{1,0:T(8,128)(2,1)S(1)}, bf16[512,128]{1,0:T(8,128)(2,1)S(1)}, u32[]{:S(2)}, u32[]{:S(2)}) %collective-permute-start.13) | collective-permute-done | bytes 131104 | tf_op jit(solution)/shard_map/ppermute | solution.py:273
  75.9 2.6 %collective-permute-start.32 = (bf16[512,128]{1,0:T(8,128)(2,1)S(1)}, bf16[512,128]{1,0:T(8,128)(2,1)S(1)}, u32[]{:S(2)}, u32[]{:S(2)}) collective-permute-start(bf16[512,128]{1,0:T(8,128)(2,1)S(1)} %get-tuple-element.69.refs_4_), channel_id=1, source_target_pairs={{0,2},{2,4},{4,6},{6,0},{1,3},{3,5},{5,7},{7,1},{8,10},{10,12},{12... | collective-permute-start | bytes 393224 | tf_op jit(solution)/shard_map/ppermute | solution.py:273
  78.5 8.2 %collective-permute-done.32.refs_5_ = bf16[512,128]{1,0:T(8,128)(2,1)S(1)} collective-permute-done((bf16[512,128]{1,0:T(8,128)(2,1)S(1)}, bf16[512,128]{1,0:T(8,128)(2,1)S(1)}, u32[]{:S(2)}, u32[]{:S(2)}) %collective-permute-start.32) | collective-permute-done | bytes 131104 | tf_op jit(solution)/shard_map/ppermute | solution.py:273
  86.7 2.2 %collective-permute-start.33 = (bf16[512,128]{1,0:T(8,128)(2,1)S(1)}, bf16[512,128]{1,0:T(8,128)(2,1)S(1)}, u32[]{:S(2)}, u32[]{:S(2)}) collective-permute-start(bf16[512,128]{1,0:T(8,128)(2,1)S(1)} %get-tuple-element.69.refs_4_), channel_id=1, source_target_pairs={{0,4},{2,6},{4,0},{6,2},{1,5},{3,7},{5,1},{7,3},{8,12},{10,14},{12... | collective-permute-start | bytes 393224 | tf_op jit(solution)/shard_map/ppermute | solution.py:273
  88.9 2.3 %collective-permute-start.34 = (bf16[512,128]{1,0:T(8,128)(2,1)S(1)}, bf16[512,128]{1,0:T(8,128)(2,1)S(1)}, u32[]{:S(2)}, u32[]{:S(2)}) collective-permute-start(bf16[512,128]{1,0:T(8,128)(2,1)S(1)} %get-tuple-element.69.refs_4_), channel_id=1, source_target_pairs={{0,6},{2,0},{4,2},{6,4},{1,7},{3,1},{5,3},{7,5},{8,14},{10,8},{12,... | collective-permute-start | bytes 393224 | tf_op jit(solution)/shard_map/ppermute | solution.py:273
  91.3 3.3 %collective-permute-done.33.refs_6_ = bf16[512,128]{1,0:T(8,128)(2,1)S(1)} collective-permute-done((bf16[512,128]{1,0:T(8,128)(2,1)S(1)}, bf16[512,128]{1,0:T(8,128)(2,1)S(1)}, u32[]{:S(2)}, u32[]{:S(2)}) %collective-permute-start.33) | collective-permute-done | bytes 131104 | tf_op jit(solution)/shard_map/ppermute | solution.py:273
  94.6 2.6 %collective-permute-start.21 = (bf16[512,512]{1,0:T(8,128)(2,1)S(1)}, bf16[512,512]{1,0:T(8,128)(2,1)S(1)}, u32[]{:S(2)}, u32[]{:S(2)}) collective-permute-start(bf16[512,512]{1,0:T(8,128)(2,1)S(1)} %slice_bitcast_fusion), channel_id=1, source_target_pairs={{0,6},{2,0},{4,2},{6,4},{1,7},{3,1},{5,3},{7,5},{8,14},{10,8},{12,... | collective-permute-start | bytes 1572872 | tf_op jit(solution)/shard_map/ppermute | solution.py:273
  98.0 18.3 %collective-permute-done.29.refs_1_ = bf16[512,1024]{1,0:T(8,128)(2,1)S(1)} collective-permute-done((bf16[512,1024]{1,0:T(8,128)(2,1)S(1)}, bf16[512,1024]{1,0:T(8,128)(2,1)S(1)}, u32[]{:S(2)}, u32[]{:S(2)}) %collective-permute-start.29) | collective-permute-done | bytes 1048608 | tf_op jit(solution)/shard_map/ppermute | solution.py:273
  116.2 2.5 %collective-permute-start.42 = (bf16[512,128]{1,0:T(8,128)(2,1)S(1)}, bf16[512,128]{1,0:T(8,128)(2,1)S(1)}, u32[]{:S(2)}, u32[]{:S(2)}) collective-permute-start(bf16[512,128]{1,0:T(8,128)(2,1)S(1)} %shard_map.124.refs_8_.refs_4_), channel_id=1, source_target_pairs={{0,2},{2,4},{4,6},{6,0},{1,3},{3,5},{5,7},{7,1},{8,10},{10,12},{12... | collective-permute-start | bytes 393224 | tf_op jit(solution)/shard_map/ppermute | solution.py:273
  118.7 2.3 %collective-permute-start.44 = (bf16[512,128]{1,0:T(8,128)(2,1)S(1)}, bf16[512,128]{1,0:T(8,128)(2,1)S(1)}, u32[]{:S(2)}, u32[]{:S(2)}) collective-permute-start(bf16[512,128]{1,0:T(8,128)(2,1)S(1)} %shard_map.124.refs_8_.refs_4_), channel_id=1, source_target_pairs={{0,6},{2,0},{4,2},{6,4},{1,7},{3,1},{5,3},{7,5},{8,14},{10,8},{12,... | collective-permute-start | bytes 393224 | tf_op jit(solution)/shard_map/ppermute | solution.py:273
  122.0 3.2 %collective-permute-done.43.refs_6_ = bf16[512,128]{1,0:T(8,128)(2,1)S(1)} collective-permute-done((bf16[512,128]{1,0:T(8,128)(2,1)S(1)}, bf16[512,128]{1,0:T(8,128)(2,1)S(1)}, u32[]{:S(2)}, u32[]{:S(2)}) %collective-permute-start.43) | collective-permute-done | bytes 131104 | tf_op jit(solution)/shard_map/ppermute | solution.py:273
  129.1 8.0 %collective-permute-done.15.refs_1_ = bf16[6,128,128]{2,1,0:T(8,128)(2,1)S(1)} collective-permute-done((bf16[6,128,128]{2,1,0:T(8,128)(2,1)S(1)}, bf16[6,128,128]{2,1,0:T(8,128)(2,1)S(1)}, u32[]{:S(2)}, u32[]{:S(2)}) %collective-permute-start.15) | collective-permute-done | bytes 196640 | tf_op jit(solution)/shard_map/ppermute | solution.py:273
  140.5 2.9 %collective-permute-start.38 = (bf16[128,512]{1,0:T(8,128)(2,1)S(1)}, bf16[128,512]{1,0:T(8,128)(2,1)S(1)}, u32[]{:S(2)}, u32[]{:S(2)}) collective-permute-start(bf16[128,512]{1,0:T(8,128)(2,1)S(1)} %shard_map.130.refs_0_), channel_id=1, source_target_pairs={{0,24},{8,0},{16,8},{24,16},{1,25},{9,1},{17,9},{25,17},{2,26},{10... | collective-permute-start | bytes 393224 | tf_op jit(solution)/shard_map/ppermute | solution.py:273
  145.6 2.4 %collective-permute-done.38.refs_3_ = bf16[128,512]{1,0:T(8,128)(2,1)S(1)} collective-permute-done((bf16[128,512]{1,0:T(8,128)(2,1)S(1)}, bf16[128,512]{1,0:T(8,128)(2,1)S(1)}, u32[]{:S(2)}, u32[]{:S(2)}) %collective-permute-start.38) | collective-permute-done | bytes 131104 | tf_op jit(solution)/shard_map/ppermute | solution.py:273
  148.1 4.3 %collective-permute-done.46.refs_1_ = bf16[128,512]{1,0:T(8,128)(2,1)S(1)} collective-permute-done((bf16[128,512]{1,0:T(8,128)(2,1)S(1)}, bf16[128,512]{1,0:T(8,128)(2,1)S(1)}, u32[]{:S(2)}, u32[]{:S(2)}) %collective-permute-start.46) | collective-permute-done | bytes 131104 | tf_op jit(solution)/shard_map/ppermute | solution.py:273
  153.3 5.0 %collective-permute-done.48.refs_3_ = bf16[128,512]{1,0:T(8,128)(2,1)S(1)} collective-permute-done((bf16[128,512]{1,0:T(8,128)(2,1)S(1)}, bf16[128,512]{1,0:T(8,128)(2,1)S(1)}, u32[]{:S(2)}, u32[]{:S(2)}) %collective-permute-start.48) | collective-permute-done | bytes 131104 | tf_op jit(solution)/shard_map/ppermute | solution.py:273
  158.3 6.3 %collective-permute-done.39.refs_1_ = bf16[512,128]{1,0:T(8,128)(2,1)S(1)} collective-permute-done((bf16[512,128]{1,0:T(8,128)(2,1)S(1)}, bf16[512,128]{1,0:T(8,128)(2,1)S(1)}, u32[]{:S(2)}, u32[]{:S(2)}) %collective-permute-start.39) | collective-permute-done | bytes 131104 | tf_op jit(solution)/shard_map/ppermute | solution.py:273
  164.6 6.5 %collective-permute-done.40.refs_2_ = bf16[512,128]{1,0:T(8,128)(2,1)S(1)} collective-permute-done((bf16[512,128]{1,0:T(8,128)(2,1)S(1)}, bf16[512,128]{1,0:T(8,128)(2,1)S(1)}, u32[]{:S(2)}, u32[]{:S(2)}) %collective-permute-start.40) | collective-permute-done | bytes 131104 | tf_op jit(solution)/shard_map/ppermute | solution.py:273
  172.1 3.9 %collective-permute-done.41.refs_3_ = bf16[512,128]{1,0:T(8,128)(2,1)S(1)} collective-permute-done((bf16[512,128]{1,0:T(8,128)(2,1)S(1)}, bf16[512,128]{1,0:T(8,128)(2,1)S(1)}, u32[]{:S(2)}, u32[]{:S(2)}) %collective-permute-start.41) | collective-permute-done | bytes 131104 | tf_op jit(solution)/shard_map/ppermute | solution.py:273
  176.0 6.7 %collective-permute-done.49.refs_1_ = bf16[512,128]{1,0:T(8,128)(2,1)S(1)} collective-permute-done((bf16[512,128]{1,0:T(8,128)(2,1)S(1)}, bf16[512,128]{1,0:T(8,128)(2,1)S(1)}, u32[]{:S(2)}, u32[]{:S(2)}) %collective-permute-start.49) | collective-permute-done | bytes 131104 | tf_op jit(solution)/shard_map/ppermute | solution.py:273
  183.1 6.1 %collective-permute-done.50.refs_2_ = bf16[512,128]{1,0:T(8,128)(2,1)S(1)} collective-permute-done((bf16[512,128]{1,0:T(8,128)(2,1)S(1)}, bf16[512,128]{1,0:T(8,128)(2,1)S(1)}, u32[]{:S(2)}, u32[]{:S(2)}) %collective-permute-start.50) | collective-permute-done | bytes 131104 | tf_op jit(solution)/shard_map/ppermute | solution.py:273
  189.2 2.7 %collective-permute-start.51 = (bf16[512,128]{1,0:T(8,128)(2,1)S(1)}, bf16[512,128]{1,0:T(8,128)(2,1)S(1)}, u32[]{:S(2)}, u32[]{:S(2)}) collective-permute-start(bf16[512,128]{1,0:T(8,128)(2,1)S(1)} %shard_map.135.refs_0_), channel_id=1, source_target_pairs={{0,96},{32,0},{64,32},{96,64},{1,97},{33,1},{65,33},{97,65},{2,98}... | collective-permute-start | bytes 393224 | tf_op jit(solution)/shard_map/ppermute | solution.py:273
  191.9 2.9 %shard_map.126 = bf16[128,2048]{1,0:T(8,128)(2,1)} custom-call(bf16[6,128,128]{2,1,0:T(8,128)(2,1)S(1)} %get-tuple-element.61.refs_0_, bf16[6,128,128]{2,1,0:T(8,128)(2,1)S(1)} %collective-permute-done.15.refs_1_, bf16[6,128,128]{2,1,0:T(8,128)(2,1)S(1)} %collective-permute-done.16.refs_2_, bf16[6,128,128]{2,1,0:T(8,128)(2,1)S(1)} %collective-permute-done.17.refs_3_, ...), custom_call_target="tpu_custom_call" | custom-call | bytes 1048576 | tf_op jit(solution)/shard_map/pallas_call | solution.py:51
  197.0 3.8 %shard_map.127 = bf16[128,4096]{1,0:T(8,128)(2,1)} custom-call(bf16[6,128,128]{2,1,0:T(8,128)(2,1)S(1)} %get-tuple-element.61.refs_0_, bf16[6,128,128]{2,1,0:T(8,128)(2,1)S(1)} %collective-permute-done.15.refs_1_, bf16[6,128,128]{2,1,0:T(8,128)(2,1)S(1)} %collective-permute-done.16.refs_2_, bf16[6,128,128]{2,1,0:T(8,128)(2,1)S(1)} %collective-permute-done.17.refs_3_, ...), custom_call_target="tpu_custom_call" | custom-call | flops 1073741824 | bytes 9437184 | tf_op jit(solution)/shard_map/pallas_call | solution.py:51
  (126 shorter events, 50.5 us)
Async XLA Ops:
  6.0 21.9 %collective-permute-start = (bf16[2,512,128]{2,1,0:T(8,128)(2,1)S(1)}, bf16[2,512,128]{2,1,0:T(8,128)(2,1)S(1)}, u32[]{:S(2)}, u32[]{:S(2)}) collective-permute-start(bf16[2,512,128]{2,1,0:T(8,128)(2,1)S(1)} %get-tuple-element.40), channel_id=1, source_target_pairs={{0,32},{32,64},{64,96},{96,0},{1,33},{33,65},{65,97},{97,1},{2,34}... | collective-permute-start | bytes 786440 | tf_op jit(solution)/shard_map/ppermute | solution.py:273
  10.0 8.5 %collective-permute-start.3 = (bf16[3,128,128]{2,1,0:T(8,128)(2,1)S(1)}, bf16[3,128,128]{2,1,0:T(8,128)(2,1)S(1)}, u32[]{:S(2)}, u32[]{:S(2)}) collective-permute-start(bf16[3,128,128]{2,1,0:T(8,128)(2,1)S(1)} %get-tuple-element.44), channel_id=1, source_target_pairs={{0,32},{32,64},{64,96},{96,0},{1,33},{33,65},{65,97},{97,1},{2,34}... | collective-permute-start | bytes 294920 | tf_op jit(solution)/shard_map/ppermute | solution.py:273
  12.0 10.9 %collective-permute-start.4 = (bf16[3,128,128]{2,1,0:T(8,128)(2,1)S(1)}, bf16[3,128,128]{2,1,0:T(8,128)(2,1)S(1)}, u32[]{:S(2)}, u32[]{:S(2)}) collective-permute-start(bf16[3,128,128]{2,1,0:T(8,128)(2,1)S(1)} %get-tuple-element.45), channel_id=1, source_target_pairs={{0,64},{32,96},{64,0},{96,32},{1,65},{33,97},{65,1},{97,33},{2,66}... | collective-permute-start | bytes 294920 | tf_op jit(solution)/shard_map/ppermute | solution.py:273
  13.7 9.7 %collective-permute-start.5 = (bf16[3,128,128]{2,1,0:T(8,128)(2,1)S(1)}, bf16[3,128,128]{2,1,0:T(8,128)(2,1)S(1)}, u32[]{:S(2)}, u32[]{:S(2)}) collective-permute-start(bf16[3,128,128]{2,1,0:T(8,128)(2,1)S(1)} %get-tuple-element.46), channel_id=1, source_target_pairs={{0,96},{32,0},{64,32},{96,64},{1,97},{33,1},{65,33},{97,65},{2,98}... | collective-permute-start | bytes 294920 | tf_op jit(solution)/shard_map/ppermute | solution.py:273
  16.3 14.3 %collective-permute-start.1 = (bf16[2,512,128]{2,1,0:T(8,128)(2,1)S(1)}, bf16[2,512,128]{2,1,0:T(8,128)(2,1)S(1)}, u32[]{:S(2)}, u32[]{:S(2)}) collective-permute-start(bf16[2,512,128]{2,1,0:T(8,128)(2,1)S(1)} %get-tuple-element.41), channel_id=1, source_target_pairs={{0,64},{32,96},{64,0},{96,32},{1,65},{33,97},{65,1},{97,33},{2,66}... | collective-permute-start | bytes 786440 | tf_op jit(solution)/shard_map/ppermute | solution.py:273
  18.5 12.6 %collective-permute-start.2 = (bf16[2,512,128]{2,1,0:T(8,128)(2,1)S(1)}, bf16[2,512,128]{2,1,0:T(8,128)(2,1)S(1)}, u32[]{:S(2)}, u32[]{:S(2)}) collective-permute-start(bf16[2,512,128]{2,1,0:T(8,128)(2,1)S(1)} %get-tuple-element.42), channel_id=1, source_target_pairs={{0,96},{32,0},{64,32},{96,64},{1,97},{33,1},{65,33},{97,65},{2,98}... | collective-permute-start | bytes 786440 | tf_op jit(solution)/shard_map/ppermute | solution.py:273
  23.5 10.3 %collective-permute-start.6 = (bf16[2,512,128]{2,1,0:T(8,128)(2,1)S(1)}, bf16[2,512,128]{2,1,0:T(8,128)(2,1)S(1)}, u32[]{:S(2)}, u32[]{:S(2)}) collective-permute-start(bf16[2,512,128]{2,1,0:T(8,128)(2,1)S(1)} %get-tuple-element.47.refs_4_), channel_id=1, source_target_pairs={{0,8},{8,16},{16,24},{24,0},{1,9},{9,17},{17,25},{25,1},{2,10},{10... | collective-permute-start | bytes 786440 | tf_op jit(solution)/shard_map/ppermute | solution.py:273
  25.1 11.5 %collective-permute-start.7 = (bf16[2,512,128]{2,1,0:T(8,128)(2,1)S(1)}, bf16[2,512,128]{2,1,0:T(8,128)(2,1)S(1)}, u32[]{:S(2)}, u32[]{:S(2)}) collective-permute-start(bf16[2,512,128]{2,1,0:T(8,128)(2,1)S(1)} %get-tuple-element.47.refs_4_), channel_id=1, source_target_pairs={{0,16},{8,24},{16,0},{24,8},{1,17},{9,25},{17,1},{25,9},{2,18},{10... | collective-permute-start | bytes 786440 | tf_op jit(solution)/shard_map/ppermute | solution.py:273
  27.8 9.6 %collective-permute-start.8 = (bf16[2,512,128]{2,1,0:T(8,128)(2,1)S(1)}, bf16[2,512,128]{2,1,0:T(8,128)(2,1)S(1)}, u32[]{:S(2)}, u32[]{:S(2)}) collective-permute-start(bf16[2,512,128]{2,1,0:T(8,128)(2,1)S(1)} %get-tuple-element.47.refs_4_), channel_id=1, source_target_pairs={{0,24},{8,0},{16,8},{24,16},{1,25},{9,1},{17,9},{25,17},{2,26},{10... | collective-permute-start | bytes 786440 | tf_op jit(solution)/shard_map/ppermute | solution.py:273
  30.6 45.3 %collective-permute-start.20 = (bf16[2,512,512]{2,1,0:T(8,128)(2,1)S(1)}, bf16[2,512,512]{2,1,0:T(8,128)(2,1)S(1)}, u32[]{:S(2)}, u32[]{:S(2)}) collective-permute-start(bf16[2,512,512]{2,1,0:T(8,128)(2,1)S(1)} %pad_maximum_fusion.refs_4_), channel_id=1, source_target_pairs={{0,6},{2,0},{4,2},{6,4},{1,7},{3,1},{5,3},{7,5},{8,14},{10,8},{12,... | collective-permute-start | bytes 3145736 | tf_op jit(solution)/shard_map/ppermute | solution.py:273
  31.1 21.5 %collective-permute-start.26 = (bf16[128,1024]{1,0:T(8,128)(2,1)S(1)}, bf16[128,1024]{1,0:T(8,128)(2,1)S(1)}, u32[]{:S(2)}, u32[]{:S(2)}) collective-permute-start(bf16[128,1024]{1,0:T(8,128)(2,1)S(1)} %get-tuple-element.66), channel_id=1, source_target_pairs={{0,2},{2,4},{4,6},{6,0},{1,3},{3,5},{5,7},{7,1},{8,10},{10,12},{12... | collective-permute-start | bytes 786440 | tf_op jit(solution)/shard_map/ppermute | solution.py:273
  33.8 27.6 %collective-permute-start.27 = (bf16[128,1024]{1,0:T(8,128)(2,1)S(1)}, bf16[128,1024]{1,0:T(8,128)(2,1)S(1)}, u32[]{:S(2)}, u32[]{:S(2)}) collective-permute-start(bf16[128,1024]{1,0:T(8,128)(2,1)S(1)} %get-tuple-element.67), channel_id=1, source_target_pairs={{0,4},{2,6},{4,0},{6,2},{1,5},{3,7},{5,1},{7,3},{8,12},{10,14},{12... | collective-permute-start | bytes 786440 | tf_op jit(solution)/shard_map/ppermute | solution.py:273
  36.6 26.5 %collective-permute-start.28 = (bf16[128,1024]{1,0:T(8,128)(2,1)S(1)}, bf16[128,1024]{1,0:T(8,128)(2,1)S(1)}, u32[]{:S(2)}, u32[]{:S(2)}) collective-permute-start(bf16[128,1024]{1,0:T(8,128)(2,1)S(1)} %get-tuple-element.68), channel_id=1, source_target_pairs={{0,6},{2,0},{4,2},{6,4},{1,7},{3,1},{5,3},{7,5},{8,14},{10,8},{12,... | collective-permute-start | bytes 786440 | tf_op jit(solution)/shard_map/ppermute | solution.py:273
  51.1 13.6 %collective-permute-start.9 = (bf16[512,128]{1,0:T(8,128)(2,1)S(1)}, bf16[512,128]{1,0:T(8,128)(2,1)S(1)}, u32[]{:S(2)}, u32[]{:S(2)}) collective-permute-start(bf16[512,128]{1,0:T(8,128)(2,1)S(1)} %get-tuple-element.49), channel_id=1, source_target_pairs={{0,24},{8,0},{16,8},{24,16},{1,25},{9,1},{17,9},{25,17},{2,26},{10... | collective-permute-start | bytes 393224 | tf_op jit(solution)/shard_map/ppermute | solution.py:273
  52.6 14.6 %collective-permute-start.10 = (bf16[512,128]{1,0:T(8,128)(2,1)S(1)}, bf16[512,128]{1,0:T(8,128)(2,1)S(1)}, u32[]{:S(2)}, u32[]{:S(2)}) collective-permute-start(bf16[512,128]{1,0:T(8,128)(2,1)S(1)} %get-tuple-element.50), channel_id=1, source_target_pairs={{0,16},{8,24},{16,0},{24,8},{1,17},{9,25},{17,1},{25,9},{2,18},{10... | collective-permute-start | bytes 393224 | tf_op jit(solution)/shard_map/ppermute | solution.py:273
  63.1 25.8 %collective-permute-start.18 = (bf16[2,512,512]{2,1,0:T(8,128)(2,1)S(1)}, bf16[2,512,512]{2,1,0:T(8,128)(2,1)S(1)}, u32[]{:S(2)}, u32[]{:S(2)}) collective-permute-start(bf16[2,512,512]{2,1,0:T(8,128)(2,1)S(1)} %pad_maximum_fusion.refs_4_), channel_id=1, source_target_pairs={{0,2},{2,4},{4,6},{6,0},{1,3},{3,5},{5,7},{7,1},{8,10},{10,12},{12... | collective-permute-start | bytes 3145736 | tf_op jit(solution)/shard_map/ppermute | solution.py:273
  69.8 46.5 %collective-permute-start.29 = (bf16[512,1024]{1,0:T(8,128)(2,1)S(1)}, bf16[512,1024]{1,0:T(8,128)(2,1)S(1)}, u32[]{:S(2)}, u32[]{:S(2)}) collective-permute-start(bf16[512,1024]{1,0:T(8,128)(2,1)S(1)} %constant_dynamic-update-slice_fusion.refs_0_), channel_id=1, source_target_pairs={{0,32},{32,64},{64,96},{96,0},{1,33},{33,65},{65,97},{97,1},{2,34}... | collective-permute-start | bytes 3145736 | tf_op jit(solution)/shard_map/ppermute | solution.py:273
  73.7 45.1 %collective-permute-start.30 = (bf16[512,1024]{1,0:T(8,128)(2,1)S(1)}, bf16[512,1024]{1,0:T(8,128)(2,1)S(1)}, u32[]{:S(2)}, u32[]{:S(2)}) collective-permute-start(bf16[512,1024]{1,0:T(8,128)(2,1)S(1)} %constant_dynamic-update-slice_fusion.refs_0_), channel_id=1, source_target_pairs={{0,64},{32,96},{64,0},{96,32},{1,65},{33,97},{65,1},{97,33},{2,66}... | collective-permute-start | bytes 3145736 | tf_op jit(solution)/shard_map/ppermute | solution.py:273
  75.0 43.8 %collective-permute-start.31 = (bf16[512,1024]{1,0:T(8,128)(2,1)S(1)}, bf16[512,1024]{1,0:T(8,128)(2,1)S(1)}, u32[]{:S(2)}, u32[]{:S(2)}) collective-permute-start(bf16[512,1024]{1,0:T(8,128)(2,1)S(1)} %constant_dynamic-update-slice_fusion.refs_0_), channel_id=1, source_target_pairs={{0,96},{32,0},{64,32},{96,64},{1,97},{33,1},{65,33},{97,65},{2,98}... | collective-permute-start | bytes 3145736 | tf_op jit(solution)/shard_map/ppermute | solution.py:273
  75.9 10.9 %collective-permute-start.32 = (bf16[512,128]{1,0:T(8,128)(2,1)S(1)}, bf16[512,128]{1,0:T(8,128)(2,1)S(1)}, u32[]{:S(2)}, u32[]{:S(2)}) collective-permute-start(bf16[512,128]{1,0:T(8,128)(2,1)S(1)} %get-tuple-element.69.refs_4_), channel_id=1, source_target_pairs={{0,2},{2,4},{4,6},{6,0},{1,3},{3,5},{5,7},{7,1},{8,10},{10,12},{12... | collective-permute-start | bytes 393224 | tf_op jit(solution)/shard_map/ppermute | solution.py:273
  88.9 8.2 %collective-permute-start.34 = (bf16[512,128]{1,0:T(8,128)(2,1)S(1)}, bf16[512,128]{1,0:T(8,128)(2,1)S(1)}, u32[]{:S(2)}, u32[]{:S(2)}) collective-permute-start(bf16[512,128]{1,0:T(8,128)(2,1)S(1)} %get-tuple-element.69.refs_4_), channel_id=1, source_target_pairs={{0,6},{2,0},{4,2},{6,4},{1,7},{3,1},{5,3},{7,5},{8,14},{10,8},{12,... | collective-permute-start | bytes 393224 | tf_op jit(solution)/shard_map/ppermute | solution.py:273
  94.6 48.8 %collective-permute-start.21 = (bf16[512,512]{1,0:T(8,128)(2,1)S(1)}, bf16[512,512]{1,0:T(8,128)(2,1)S(1)}, u32[]{:S(2)}, u32[]{:S(2)}) collective-permute-start(bf16[512,512]{1,0:T(8,128)(2,1)S(1)} %slice_bitcast_fusion), channel_id=1, source_target_pairs={{0,6},{2,0},{4,2},{6,4},{1,7},{3,1},{5,3},{7,5},{8,14},{10,8},{12,... | collective-permute-start | bytes 1572872 | tf_op jit(solution)/shard_map/ppermute | solution.py:273
  97.2 46.3 %collective-permute-start.19 = (bf16[512,512]{1,0:T(8,128)(2,1)S(1)}, bf16[512,512]{1,0:T(8,128)(2,1)S(1)}, u32[]{:S(2)}, u32[]{:S(2)}) collective-permute-start(bf16[512,512]{1,0:T(8,128)(2,1)S(1)} %slice_bitcast_fusion.1), channel_id=1, source_target_pairs={{0,2},{2,4},{4,6},{6,0},{1,3},{3,5},{5,7},{7,1},{8,10},{10,12},{12... | collective-permute-start | bytes 1572872 | tf_op jit(solution)/shard_map/ppermute | solution.py:273
  126.1 10.9 %collective-permute-start.15 = (bf16[6,128,128]{2,1,0:T(8,128)(2,1)S(1)}, bf16[6,128,128]{2,1,0:T(8,128)(2,1)S(1)}, u32[]{:S(2)}, u32[]{:S(2)}) collective-permute-start(bf16[6,128,128]{2,1,0:T(8,128)(2,1)S(1)} %get-tuple-element.62), channel_id=1, source_target_pairs={{0,96},{32,0},{64,32},{96,64},{1,97},{33,1},{65,33},{97,65},{2,98}... | collective-permute-start | bytes 589832 | tf_op jit(solution)/shard_map/ppermute | solution.py:273
  128.0 9.3 %collective-permute-start.16 = (bf16[6,128,128]{2,1,0:T(8,128)(2,1)S(1)}, bf16[6,128,128]{2,1,0:T(8,128)(2,1)S(1)}, u32[]{:S(2)}, u32[]{:S(2)}) collective-permute-start(bf16[6,128,128]{2,1,0:T(8,128)(2,1)S(1)} %get-tuple-element.63), channel_id=1, source_target_pairs={{0,64},{32,96},{64,0},{96,32},{1,65},{33,97},{65,1},{97,33},{2,66}... | collective-permute-start | bytes 589832 | tf_op jit(solution)/shard_map/ppermute | solution.py:273
  128.0 12.4 %collective-permute-start.17 = (bf16[6,128,128]{2,1,0:T(8,128)(2,1)S(1)}, bf16[6,128,128]{2,1,0:T(8,128)(2,1)S(1)}, u32[]{:S(2)}, u32[]{:S(2)}) collective-permute-start(bf16[6,128,128]{2,1,0:T(8,128)(2,1)S(1)} %get-tuple-element.64), channel_id=1, source_target_pairs={{0,32},{32,64},{64,96},{96,0},{1,33},{33,65},{65,97},{97,1},{2,34}... | collective-permute-start | bytes 589832 | tf_op jit(solution)/shard_map/ppermute | solution.py:273
  143.4 8.9 %collective-permute-start.46 = (bf16[128,512]{1,0:T(8,128)(2,1)S(1)}, bf16[128,512]{1,0:T(8,128)(2,1)S(1)}, u32[]{:S(2)}, u32[]{:S(2)}) collective-permute-start(bf16[128,512]{1,0:T(8,128)(2,1)S(1)} %shard_map.134.refs_0_), channel_id=1, source_target_pairs={{0,8},{8,16},{16,24},{24,0},{1,9},{9,17},{17,25},{25,1},{2,10},{10... | collective-permute-start | bytes 393224 | tf_op jit(solution)/shard_map/ppermute | solution.py:273
  143.4 8.9 %collective-permute-start.47 = (bf16[128,512]{1,0:T(8,128)(2,1)S(1)}, bf16[128,512]{1,0:T(8,128)(2,1)S(1)}, u32[]{:S(2)}, u32[]{:S(2)}) collective-permute-start(bf16[128,512]{1,0:T(8,128)(2,1)S(1)} %shard_map.134.refs_0_), channel_id=1, source_target_pairs={{0,16},{8,24},{16,0},{24,8},{1,17},{9,25},{17,1},{25,9},{2,18},{10... | collective-permute-start | bytes 393224 | tf_op jit(solution)/shard_map/ppermute | solution.py:273
  145.0 52.0 %collective-permute-start.22 = (bf16[2,512,512]{2,1,0:T(8,128)(2,1)S(1)}, bf16[2,512,512]{2,1,0:T(8,128)(2,1)S(1)}, u32[]{:S(2)}, u32[]{:S(2)}) collective-permute-start(bf16[2,512,512]{2,1,0:T(8,128)(2,1)S(1)} %pad_maximum_fusion.refs_4_), channel_id=1, source_target_pairs={{0,1},{1,0},{2,3},{3,2},{4,5},{5,4},{6,7},{7,6},{8,9},{9,8},{10,11... | collective-permute-start | bytes 3145736 | tf_op jit(solution)/shard_map/ppermute | solution.py:273
  145.1 51.9 %collective-permute-start.23 = (bf16[2,512,512]{2,1,0:T(8,128)(2,1)S(1)}, bf16[2,512,512]{2,1,0:T(8,128)(2,1)S(1)}, u32[]{:S(2)}, u32[]{:S(2)}) collective-permute-start(bf16[2,512,512]{2,1,0:T(8,128)(2,1)S(1)} %collective-permute-done.18.refs_5_), channel_id=1, source_target_pairs={{0,1},{1,0},{2,3},{3,2},{4,5},{5,4},{6,7},{7,6},{8,9},{9,8},{10,11... | collective-permute-start | bytes 3145736 | tf_op jit(solution)/shard_map/ppermute | solution.py:273
  148.1 48.9 %collective-permute-start.25 = (bf16[2,512,512]{2,1,0:T(8,128)(2,1)S(1)}, bf16[2,512,512]{2,1,0:T(8,128)(2,1)S(1)}, u32[]{:S(2)}, u32[]{:S(2)}) collective-permute-start(bf16[2,512,512]{2,1,0:T(8,128)(2,1)S(1)} %collective-permute-done.20.refs_7_), channel_id=1, source_target_pairs={{0,1},{1,0},{2,3},{3,2},{4,5},{5,4},{6,7},{7,6},{8,9},{9,8},{10,11... | collective-permute-start | bytes 3145736 | tf_op jit(solution)/shard_map/ppermute | solution.py:273
  152.4 44.6 %collective-permute-start.24 = (bf16[2,512,512]{2,1,0:T(8,128)(2,1)S(1)}, bf16[2,512,512]{2,1,0:T(8,128)(2,1)S(1)}, u32[]{:S(2)}, u32[]{:S(2)}) collective-permute-start(bf16[2,512,512]{2,1,0:T(8,128)(2,1)S(1)} %pad_maximum_fusion.1.refs_6_), channel_id=1, source_target_pairs={{0,1},{1,0},{2,3},{3,2},{4,5},{5,4},{6,7},{7,6},{8,9},{9,8},{10,11... | collective-permute-start | bytes 3145736 | tf_op jit(solution)/shard_map/ppermute | solution.py:273
  (30 other events, 212.8 us)
